TPU v7x, 32 devices: a whole 2x2x4 slice. The times are simulated.
32 devices in a mesh: grp: 2 (over y), sp: 4 (over z), tp: 4 (over x, core).
Axes of the slice: x: 2, y: 2, z: 4, core: 2. Of those that a mesh axis runs over, the one named last changes fastest.
Arguments:
- starting_stream: bfloat16 [3072, 2048], P(('grp', 'sp'), 'tp'), parts along dimension 0, may hold values from -45 to 45
- multiplier_matrix: bfloat16 [2, 2048, 2048], P(None, 'sp', 'tp'), may hold values from -0.125 to 0.125
- memory_path_matrix: bfloat16 [2, 2048, 2048], P(None, 'sp', 'tp'), may hold values from -0.125 to 0.125
- filter_coefficients: bfloat16 [2, 4, 2048], P(None, None, 'tp'), may hold values from -3 to 3
- memory_valve_matrix: bfloat16 [2, 8, 256, 256], P(None, 'tp'), may hold values from -0.375 to 0.375
- entry_valve_matrix: bfloat16 [2, 8, 256, 256], P(None, 'tp'), may hold values from -0.375 to 0.375
- forgetting_parameters: float32 [2, 2048], P(None, 'tp'), may hold values from 3 to 15
- timestep_forgetting_multiplier: float32 [3072], P(('grp', 'sp')), parts along dimension 0, may hold values from 0.5 to 2
- spike_extra: float32 [3072, 2048], P(('grp', 'sp'), 'tp'), parts along dimension 0, may hold values from -0.7 to 0
- exit_projector_matrix: bfloat16 [2, 2048, 2048], P(None, 'tp', 'sp'), may hold values from -0.125 to 0.125
- prelude_rms_gains: float32 [2, 2048], replicated, may hold values from 0.1 to 1.9
- finishing_rms_gains: float32 [2048], P('tp'), may hold values from 0.1 to 1.9
Outputs:
- result: bfloat16 [3072, 2048], P(('grp', 'sp'), 'tp'), parts along dimension 0
There are 2 independent parts, one for each index of `grp`. A program takes and returns all parts, laid end to end along the dimension named above; an argument that names none is the same for every part. Nothing has to cross between parts.
All inputs are finite; a program needn't handle non-finite values.
Results may differ from a plain program's by a relative error of at most 0.015.
Values may be sent and summed in bfloat16 or wider, within the bound.
A program may use at most 64 MiB of HBM per device.

v0:
```python
import functools

import jax
import jax.numpy as jnp
from jax import lax
from jax.experimental import pallas as pl
from jax.experimental.pallas import tpu as pltpu
from jax.sharding import PartitionSpec as P

BLOCK_W = 256


EPSILON = 1e-06
SQUASH_POWER = 8.0


def from_behind(value, axis, steps):
    count = lax.axis_size(axis)
    first, last = (max(0, -steps), min(count, count - steps))
    return lax.ppermute(value, axis, [(source, source + steps) for source in range(first, last)])


def entering(part, axis, combine, identity):
    place = lax.axis_index(axis)
    gathered = jax.tree.map(lambda a: lax.all_gather(a, axis), part)
    state = jax.tree.map(lambda a, e: jnp.zeros_like(a) + jnp.asarray(e, a.dtype), part, identity)

    def one(lap, state):
        return combine(
            state, jax.tree.map(lambda a: lax.dynamic_index_in_dim(a, lap, 0, False), gathered)
        )

    return lax.fori_loop(0, place, one, state)


def combine_pairs(earlier, later):
    return (earlier[0] * later[0], later[0] * earlier[1] + later[1])


def gather_rows(own_cols):
    return lax.all_gather(own_cols, "tp", axis=1, tiled=True)


def on_device(
    starting_stream,
    multiplier_matrix,
    memory_path_matrix,
    filter_coefficients,
    memory_valve_matrix,
    entry_valve_matrix,
    forgetting_parameters,
    timestep_forgetting_multiplier,
    spike_extra,
    exit_projector_matrix,
    prelude_rms_gains,
    finishing_rms_gains,
):
    tok_rows = starting_stream.shape[0]
    channels = memory_path_matrix.shape[2]
    own_cols = starting_stream
    full_rows = gather_rows(starting_stream)
    for tier_number in range(memory_path_matrix.shape[0]):
        floats = full_rows.astype(jnp.float32)
        mean_square = jnp.mean(floats * floats, axis=1, keepdims=True)
        normed = (
            floats * lax.rsqrt(mean_square + EPSILON) * prelude_rms_gains[tier_number][None, :]
        ).astype(jnp.bfloat16)
        branch_acc = jnp.dot(
            normed,
            lax.all_gather(multiplier_matrix[tier_number], "sp", axis=0, tiled=True),
            preferred_element_type=jnp.float32,
        )
        recur_acc = jnp.dot(
            normed,
            lax.all_gather(memory_path_matrix[tier_number], "sp", axis=0, tiled=True),
            preferred_element_type=jnp.float32,
        )
        branch = branch_acc.astype(jnp.bfloat16)
        recurrent = recur_acc.astype(jnp.bfloat16)
        taps_now = filter_coefficients[tier_number]
        reach_back = taps_now.shape[0] - 1
        halo_rows = from_behind(recurrent[tok_rows - reach_back :], "sp", 1)
        extended = jnp.concatenate([halo_rows, recurrent], axis=0)
        conv_sum = jnp.zeros((tok_rows, channels), jnp.float32)
        for offset in range(taps_now.shape[0]):
            conv_sum = conv_sum + extended[offset : offset + tok_rows].astype(
                jnp.float32
            ) * taps_now[offset].astype(jnp.float32)
        convolved = conv_sum.astype(jnp.bfloat16)
        blocks = convolved.reshape(tok_rows, channels // BLOCK_W, BLOCK_W)
        reset_gate = jax.nn.sigmoid(
            jnp.einsum(
                "tnc,ncd->tnd",
                blocks,
                memory_valve_matrix[tier_number],
                preferred_element_type=jnp.float32,
            ).reshape(tok_rows, channels)
        )
        inject = jax.nn.sigmoid(
            jnp.einsum(
                "tnc,ncd->tnd",
                blocks,
                entry_valve_matrix[tier_number],
                preferred_element_type=jnp.float32,
            ).reshape(tok_rows, channels)
        )
        logarithmic_persistence = (
            -SQUASH_POWER
            * reset_gate
            * jax.nn.softplus(-forgetting_parameters[tier_number])[None, :]
            * timestep_forgetting_multiplier[:, None]
            + spike_extra
        )
        keep_rate = jnp.exp(logarithmic_persistence)
        driven = (
            inject
            * convolved.astype(jnp.float32)
            * jnp.sqrt(-jnp.expm1(2.0 * logarithmic_persistence))
        )
        keep_cum, state_local = lax.associative_scan(combine_pairs, (keep_rate, driven), axis=0)
        identity = (jnp.ones((channels,), jnp.float32), jnp.zeros((channels,), jnp.float32))
        carried = entering((keep_cum[-1], state_local[-1]), "sp", combine_pairs, identity)
        state_seq = state_local + keep_cum * carried[1][None, :]
        mixed_in = (jax.nn.gelu(branch.astype(jnp.float32)) * state_seq).astype(jnp.bfloat16)
        partial_value = jnp.dot(
            mixed_in,
            lax.all_gather(exit_projector_matrix[tier_number], "sp", axis=1, tiled=True),
            preferred_element_type=jnp.float32,
        )
        mixed_sum = lax.psum_scatter(
            partial_value.astype(jnp.bfloat16), "tp", scatter_dimension=1, tiled=True
        ).astype(jnp.float32)
        own_cols = (own_cols.astype(jnp.float32) + mixed_sum).astype(jnp.bfloat16)
        if tier_number + 1 < memory_path_matrix.shape[0]:
            full_rows = gather_rows(own_cols)
    floats = own_cols.astype(jnp.float32)
    full_width = floats.shape[1] * lax.axis_size("tp")
    square_sum = lax.psum(jnp.sum(floats * floats, axis=1), "tp")
    inv_rms = lax.rsqrt(square_sum / full_width + EPSILON)
    return (floats * inv_rms[:, None] * finishing_rms_gains[None, :]).astype(jnp.bfloat16)


MESH = pl.DeviceIdType.MESH
F32, BF16 = jnp.float32, jnp.bfloat16


def one_minus_exp(u):
    series = -u * (
        1 + u / 2 * (1 + u / 3 * (1 + u / 4 * (1 + u / 5 * (1 + u / 6 * (1 + u / 7)))))
    )
    return jnp.where(u > -0.35, series, 1.0 - jnp.exp(u))


def shifted(value, steps, fill):
    rows = value.shape[0]
    if steps % 8 == 0:
        top = jnp.full((steps, value.shape[1]), fill, value.dtype)
        return jnp.concatenate([top, value[: rows - steps]], axis=0)
    at = lax.broadcasted_iota(jnp.int32, value.shape, 0)
    return jnp.where(at < steps, fill, pltpu.roll(value, steps, 0))


def fused(
    sizes,
    x_ref,
    branch_w,
    memory_w,
    exit_w,
    taps_ref,
    reset_w,
    inject_w,
    rate_ref,
    mult_ref,
    spike_ref,
    gains_ref,
    final_ref,
    out_ref,
    win,
    wout,
    agx,
    xs,
    nrm,
    ext,
    halo,
    keep_s,
    state_s,
    gel_s,
    mix_s,
    part,
    from_sib,
    pair,
    from_far,
    cry_out,
    cry_in,
    hacc,
    sq_out,
    sq_in,
    sem_own,
    sem_w_recv,
    sem_up,
    sem_down,
    sem_y,
    sem_ag_send,
    sem_ag_recv,
    sem_rs_send,
    sem_rs_recv,
    sem_h,
    sem_c_send,
    sem_c_recv,
    sem_q_send,
    sem_q_recv,
):
    layers, n_sp, n_tp, n_grp, rows, chans, feats, depth, pieces = sizes
    chips = n_tp // 2
    g, s, t = lax.axis_index("grp"), lax.axis_index("sp"), lax.axis_index("tp")
    core = lax.rem(t, 2)
    chip = t // 2
    sib = chip * 2 + 1 - core
    full = n_tp * feats

    def up():
        return {"sp": s + 1}

    def down():
        return {"sp": s - 1}

    def across():
        return {"grp": 1 - g}

    barrier = pltpu.get_barrier_semaphore()
    for d in range(1, n_tp):
        pl.semaphore_signal(
            barrier, inc=1, device_id={"tp": lax.rem(t + d, n_tp)}, device_id_type=MESH
        )
    for d in range(1, n_sp):
        pl.semaphore_signal(
            barrier, inc=1, device_id={"sp": lax.rem(s + d, n_sp)}, device_id_type=MESH
        )
    pl.semaphore_signal(barrier, inc=1, device_id=across(), device_id_type=MESH)
    pl.semaphore_wait(barrier, n_tp - 1 + n_sp - 1 + 1)

    def own_block(m):
        return (memory_w, branch_w, exit_w)[m % 3].at[m // 3]

    def held(m, j):
        return win.at[2 * (m // 3) + m % 3, j] if m % 3 < 2 else wout.at[m // 3, j]

    def sent(src, m, j, half, send_sem, where):
        return pltpu.make_async_remote_copy(
            src_ref=src,
            dst_ref=held(m, j).at[half],
            send_sem=send_sem.at[m, j],
            recv_sem=sem_w_recv.at[m, j, half],
            device_id=where,
            device_id_type=MESH,
        )

    def start_own(m):
        src = own_block(m).at[g]

        @pl.when(s < n_sp - 1)
        def _():
            sent(src, m, s, g, sem_up, up()).start()

        @pl.when(s > 0)
        def _():
            sent(src, m, s, g, sem_down, down()).start()

    def keep_own(m):
        return pltpu.make_async_copy(own_block(m), held(m, s), sem_own.at[m])

    items = [(m, d) for m in range(3 * layers) for d in range(1, n_sp)]
    place = [0]

    def pump(m, d):
        @pl.when(s - d >= 0)
        def _():
            j = s - d
            src = held(m, j).at[g]
            sent(src, m, j, g, sem_up, up()).wait_recv()

            @pl.when(s < n_sp - 1)
            def _():
                sent(src, m, j, g, sem_up, up()).start()

            sent(src, m, j, g, sem_y, across()).start()

        @pl.when(s + d < n_sp)
        def _():
            j = s + d
            src = held(m, j).at[g]
            sent(src, m, j, g, sem_down, down()).wait_recv()

            @pl.when(s > 0)
            def _():
                sent(src, m, j, g, sem_down, down()).start()

            sent(src, m, j, g, sem_y, across()).start()

        if d == n_sp - 1 and m + 2 < 3 * layers:
            start_own(m + 2)

    def advance(steps):
        for m, d in items[place[0] : place[0] + steps]:
            pump(m, d)
        place[0] = min(place[0] + steps, len(items))

    def reach(m, d):
        advance(max(0, m * (n_sp - 1) + d - place[0]))

    def swapped(m, j):
        src = held(m, j).at[1 - g]
        sent(src, m, j, 1 - g, sem_y, across()).wait_recv()

    def arrived(m):
        reach(m, n_sp - 1)
        keep_own(m).wait()
        for d in range(1, n_sp):
            swapped(m, lax.rem(s + d, n_sp))

    def close_weights():
        for m in range(3 * layers):
            for j in range(n_sp):
                src = held(m, j).at[g]

                @pl.when((s < n_sp - 1) & (j <= s))
                def _():
                    sent(src, m, j, g, sem_up, up()).wait_send()

                @pl.when((s > 0) & (j >= s))
                def _():
                    sent(src, m, j, g, sem_down, down()).wait_send()

                @pl.when(j != s)
                def _():
                    sent(src, m, j, g, sem_y, across()).wait_send()

    for m in range(3 * layers):
        keep_own(m).start()

    def ag_copy(src, layer, owner, k, where):
        return pltpu.make_async_remote_copy(
            src_ref=src,
            dst_ref=agx.at[layer, owner],
            send_sem=sem_ag_send.at[layer, k],
            recv_sem=sem_ag_recv.at[layer, owner],
            device_id={"tp": where},
            device_id_type=MESH,
        )

    def ag_start(layer, src):
        for d in range(1, chips):
            ag_copy(src, layer, t, d, lax.rem(t + 2 * d, n_tp)).start()
        ag_copy(src, layer, t, 0, sib).start()

    def ag_finish(layer, src):
        for d in range(1, chips):
            owner = lax.rem(t + 2 * d, n_tp)
            block = agx.at[layer, owner]
            ag_copy(block, layer, owner, d, sib).wait_recv()
            ag_copy(block, layer, owner, chips + d, sib).start()
        ag_copy(src, layer, sib, 0, sib).wait_recv()
        for d in range(1, chips):
            owner = lax.rem(sib + 2 * d, n_tp)
            ag_copy(agx.at[layer, owner], layer, owner, d, sib).wait_recv()

    def ag_close(layer, src):
        for d in range(1, chips):
            ag_copy(src, layer, t, d, sib).wait_send()
            ag_copy(src, layer, t, chips + d, sib).wait_send()
        ag_copy(src, layer, t, 0, sib).wait_send()

    ag_start(0, x_ref)
    for m in range(2):
        start_own(m)

    step = rows // pieces

    def normalize(layer):
        def one(i, carry):
            at = pl.ds(pl.multiple_of(i * step, step), step)
            total = jnp.zeros((step, 1), F32)
            for p in range(n_tp):
                f = agx[layer, p, at].astype(F32)
                total = total + jnp.sum(f * f, axis=1, keepdims=True)
            inv = lax.rsqrt(total / full + EPSILON)
            for p in range(n_tp):
                cols = slice(p * feats, (p + 1) * feats)
                f = agx[layer, p, at].astype(F32)
                gain = gains_ref[layer : layer + 1, cols]
                nrm[at, cols] = (f * inv * gain).astype(BF16)
            return carry

        lax.fori_loop(0, pieces, one, 0)

    def project(idx):
        total = None
        for j in range(n_sp):
            term = jnp.dot(
                nrm[:, j * depth : (j + 1) * depth],
                win[idx, j].reshape(depth, chans),
                preferred_element_type=F32,
            )
            total = term if total is None else total + term
        return total.astype(BF16).astype(F32)

    def halo_copy(layer):
        return pltpu.make_async_remote_copy(
            src_ref=ext.at[layer, pl.ds(rows, 8)],
            dst_ref=halo.at[layer],
            send_sem=sem_h.at[layer, 0],
            recv_sem=sem_h.at[layer, 1],
            device_id=up(),
            device_id_type=MESH,
        )

    def carry_copy(layer, d):
        return pltpu.make_async_remote_copy(
            src_ref=cry_out.at[layer],
            dst_ref=cry_in.at[layer, s],
            send_sem=sem_c_send.at[layer, d],
            recv_sem=sem_c_recv.at[layer, s],
            device_id={"sp": s + d},
            device_id_type=MESH,
        )

    def carry_wait(layer, j):
        pltpu.make_async_remote_copy(
            src_ref=cry_out.at[layer],
            dst_ref=cry_in.at[layer, j],
            send_sem=sem_c_send.at[layer, 0],
            recv_sem=sem_c_recv.at[layer, j],
            device_id={"sp": s},
            device_id_type=MESH,
        ).wait_recv()

    def rs_copy(src, dst, layer, k, where):
        return pltpu.make_async_remote_copy(
            src_ref=src,
            dst_ref=dst,
            send_sem=sem_rs_send.at[layer, k],
            recv_sem=sem_rs_recv.at[layer, k],
            device_id={"tp": where},
            device_id_type=MESH,
        )

    def near_copy(layer, q):
        to = lax.rem(sib + 2 * q, n_tp)
        return rs_copy(part.at[layer, to], from_sib.at[layer, q], layer, q, sib)

    def far_copy(layer, q):
        where = lax.rem(t + 2 * q, n_tp)
        return rs_copy(pair.at[layer, q], from_far.at[layer, q], layer, chips + q, where)

    for layer in range(layers):
        m0 = 3 * layer
        src = x_ref if layer == 0 else xs.at[layer]
        agx[layer, t] = src[...]
        advance(1)
        ag_finish(layer, src)
        advance(1)
        normalize(layer)
        reach(m0, n_sp)
        arrived(m0)
        ext[layer, 8:] = project(2 * layer)

        @pl.when(s < n_sp - 1)
        def _():
            halo_copy(layer).start()

        advance(1)

        @pl.when(s == 0)
        def _():
            halo[layer] = jnp.zeros((8, chans), F32)

        @pl.when(s > 0)
        def _():
            halo_copy(layer).wait_recv()

        ext[layer, :8] = halo[layer]
        n_taps = taps_ref.shape[1]
        base = 8 - (n_taps - 1)
        for b in range(chans // BLOCK_W):
            cols = slice(b * BLOCK_W, (b + 1) * BLOCK_W)
            conv = jnp.zeros((rows, BLOCK_W), F32)
            for k in range(n_taps):
                tap = taps_ref[layer, k : k + 1, cols].astype(F32)
                conv = conv + ext[layer, base + k : base + k + rows, cols] * tap
            conv = conv.astype(BF16)
            reset = jax.nn.sigmoid(
                jnp.dot(conv, reset_w[layer, b], preferred_element_type=F32)
            )
            inject = jax.nn.sigmoid(
                jnp.dot(conv, inject_w[layer, b], preferred_element_type=F32)
            )
            log_keep = (
                reset * rate_ref[layer : layer + 1, cols] * mult_ref[...]
                + spike_ref[:, cols]
            )
            keep = jnp.exp(log_keep)
            state = inject * conv.astype(F32) * jnp.sqrt(one_minus_exp(2.0 * log_keep))
            lag = 1
            while lag < rows:
                state = keep * shifted(state, lag, 0.0) + state
                keep = keep * shifted(keep, lag, 1.0)
                lag *= 2
            keep_s[:, cols] = keep
            state_s[:, cols] = state
            cry_out[layer, 0:1, cols] = keep[rows - 1 :]
            cry_out[layer, 1:2, cols] = state[rows - 1 :]
            advance(1)
        for d in range(1, n_sp):

            @pl.when(s + d < n_sp)
            def _():
                carry_copy(layer, d).start()

        reach(m0 + 2, min(2, n_sp - 1))
        arrived(m0 + 1)
        gel_s[...] = jax.nn.gelu(project(2 * layer + 1))
        hacc[...] = jnp.zeros((1, chans), F32)
        for j in range(n_sp - 1):

            @pl.when(j < s)
            def _():
                carry_wait(layer, j)
                hacc[...] = cry_in[layer, j, 0:1] * hacc[...] + cry_in[layer, j, 1:2]

        mix_s[...] = (
            gel_s[...] * (state_s[...] + keep_s[...] * hacc[...])
        ).astype(BF16)
        def chips_on(j):
            return lax.rem(j // 2 - chip + chips, chips)

        def product(j):
            part[layer, j] = jnp.dot(
                mix_s[...],
                wout[layer, j].reshape(chans, depth),
                preferred_element_type=F32,
            ).astype(BF16)

            @pl.when(lax.rem(j, 2) != core)
            def _():
                near_copy(layer, chips_on(j)).start()

        def pass_on(j):
            q = chips_on(j)

            @pl.when((lax.rem(j, 2) == core) & (q != 0))
            def _():
                near_copy(layer, q).wait_recv()
                pair[layer, q] = (
                    part[layer, j].astype(F32) + from_sib[layer, q].astype(F32)
                ).astype(BF16)
                far_copy(layer, q).start()

        m = m0 + 2
        keep_own(m).wait()
        product(s)
        for d in range(1, n_sp):
            reach(m, d)
            if d > 1:
                advance(1)

            @pl.when(s - d >= 0)
            def _():
                swapped(m, s - d)
                product(s - d)

            @pl.when(s + d < n_sp)
            def _():
                swapped(m, s + d)
                product(s + d)

            if d == 1:
                pass_on(s)
            else:
                for j in (s - d + 1, s + d - 1):

                    @pl.when((j >= 0) & (j < n_sp))
                    def _():
                        pass_on(j)

        for j in (s - n_sp + 1, s + n_sp - 1):

            @pl.when((j >= 0) & (j < n_sp))
            def _():
                pass_on(j)

        advance(1)
        near_copy(layer, 0).wait_recv()
        mixed = part[layer, t].astype(F32) + from_sib[layer, 0].astype(F32)
        for q in range(1, chips):
            far_copy(layer, q).wait_recv()
            mixed = mixed + from_far[layer, q].astype(F32)
        fresh = (src[...].astype(F32) + mixed).astype(BF16)
        xs[layer + 1] = fresh
        if layer + 1 < layers:
            ag_start(layer + 1, xs.at[layer + 1])

    last = xs[layers].astype(F32)
    square = jnp.sum(last * last, axis=1, keepdims=True)
    sq_out[...] = jnp.broadcast_to(square, (rows, 128)).T[0:8]

    def sq_copy(d):
        return pltpu.make_async_remote_copy(
            src_ref=sq_out,
            dst_ref=sq_in.at[d],
            send_sem=sem_q_send.at[d],
            recv_sem=sem_q_recv.at[d],
            device_id={"tp": lax.rem(t + d, n_tp)},
            device_id_type=MESH,
        )

    for d in range(1, n_tp):
        sq_copy(d).start()
    total = sq_out[0:1]
    for d in range(1, n_tp):
        sq_copy(d).wait_recv()
        total = total + sq_in[d, 0:1]
    inv = lax.rsqrt(total / full + EPSILON)
    inv = jnp.broadcast_to(inv, (128, rows)).T[:, 0:1]
    out_ref[...] = (xs[layers].astype(F32) * inv * final_ref[...]).astype(BF16)

    close_weights()
    for layer in range(layers):
        ag_close(layer, x_ref if layer == 0 else xs.at[layer])

        @pl.when(s < n_sp - 1)
        def _():
            halo_copy(layer).wait_send()

        for d in range(1, n_sp):

            @pl.when(s + d < n_sp)
            def _():
                carry_copy(layer, d).wait_send()

        for q in range(chips):
            near_copy(layer, q).wait_send()
        for q in range(1, chips):
            far_copy(layer, q).wait_send()
    for d in range(1, n_tp):
        sq_copy(d).wait_send()


def in_one_kernel(
    sizes_of,
    starting_stream,
    multiplier_matrix,
    memory_path_matrix,
    filter_coefficients,
    memory_valve_matrix,
    entry_valve_matrix,
    forgetting_parameters,
    timestep_forgetting_multiplier,
    spike_extra,
    exit_projector_matrix,
    prelude_rms_gains,
    finishing_rms_gains,
):
    n_grp, n_sp, n_tp = sizes_of
    rows, feats = starting_stream.shape
    layers, depth, chans = memory_path_matrix.shape
    pieces = rows // 128 if rows % 128 == 0 else 1
    sizes = (layers, n_sp, n_tp, n_grp, rows, chans, feats, depth, pieces)
    chips = n_tp // 2
    half_in = (layers, 2, depth // 2, chans)
    half_out = (layers, 2, chans // 2, depth)
    rate = -SQUASH_POWER * jax.nn.softplus(-forgetting_parameters)
    vmem = pl.BlockSpec(memory_space=pltpu.VMEM)
    hbm = pl.BlockSpec(memory_space=pl.ANY)
    count = 3 * layers
    dma = pltpu.SemaphoreType.DMA
    return pl.pallas_call(
        functools.partial(fused, sizes),
        out_shape=jax.ShapeDtypeStruct((rows, feats), BF16),
        in_specs=[vmem, hbm, hbm, hbm] + [vmem] * 8,
        out_specs=vmem,
        scratch_shapes=[
            pltpu.VMEM((2 * layers, n_sp, 2, depth // 2, chans), BF16),
            pltpu.VMEM((layers, n_sp, 2, chans // 2, depth), BF16),
            pltpu.VMEM((layers, n_tp, rows, feats), BF16),
            pltpu.VMEM((layers + 1, rows, feats), BF16),
            pltpu.VMEM((rows, n_tp * feats), BF16),
            pltpu.VMEM((layers, 8 + rows, chans), F32),
            pltpu.VMEM((layers, 8, chans), F32),
            pltpu.VMEM((rows, chans), F32),
            pltpu.VMEM((rows, chans), F32),
            pltpu.VMEM((rows, chans), F32),
            pltpu.VMEM((rows, chans), BF16),
            pltpu.VMEM((layers, n_tp, rows, feats), BF16),
            pltpu.VMEM((layers, chips, rows, feats), BF16),
            pltpu.VMEM((layers, chips, rows, feats), BF16),
            pltpu.VMEM((layers, chips, rows, feats), BF16),
            pltpu.VMEM((layers, 2, chans), F32),
            pltpu.VMEM((layers, n_sp, 2, chans), F32),
            pltpu.VMEM((1, chans), F32),
            pltpu.VMEM((8, rows), F32),
            pltpu.VMEM((n_tp, 8, rows), F32),
            dma((count,)),
            dma((count, n_sp, 2)),
            dma((count, n_sp)),
            dma((count, n_sp)),
            dma((count, n_sp)),
            dma((layers, 2 * chips)),
            dma((layers, n_tp)),
            dma((layers, 2 * chips)),
            dma((layers, 2 * chips)),
            dma((layers, 2)),
            dma((layers, n_sp)),
            dma((layers, n_sp)),
            dma((n_tp,)),
            dma((n_tp,)),
        ],
        compiler_params=pltpu.CompilerParams(
            collective_id=0, has_side_effects=True, vmem_limit_bytes=60 * 2**20
        ),
    )(
        starting_stream,
        multiplier_matrix.reshape(half_in),
        memory_path_matrix.reshape(half_in),
        exit_projector_matrix.reshape(half_out),
        filter_coefficients,
        memory_valve_matrix,
        entry_valve_matrix,
        rate,
        timestep_forgetting_multiplier.reshape(rows, 1),
        spike_extra,
        prelude_rms_gains,
        finishing_rms_gains.reshape(1, feats),
    )


def on_each(sizes_of, *arrays):
    stream, memory = arrays[0], arrays[2]
    n_grp, n_sp, n_tp = sizes_of
    rows, feats = stream.shape
    depth, chans = memory.shape[1:]
    fits = (
        n_grp == 2
        and n_sp > 1
        and n_tp % 2 == 0
        and rows % 128 == 0
        and depth % 128 == 0
        and feats % 128 == 0
        and chans % BLOCK_W == 0
        and depth == feats
        and n_sp == n_tp
    )
    if fits:
        return in_one_kernel(sizes_of, *arrays)
    return on_device(*arrays)


def solution(mesh):
    sizes_of = tuple(mesh.shape[axis] for axis in ("grp", "sp", "tp"))
    body = functools.partial(on_each, sizes_of)
    return jax.shard_map(
        body,
        mesh=mesh,
        in_specs=(
            P(("grp", "sp"), "tp"),
            P(None, "sp", "tp"),
            P(None, "sp", "tp"),
            P(None, None, "tp"),
            P(None, "tp", None, None),
            P(None, "tp", None, None),
            P(None, "tp"),
            P(("grp", "sp")),
            P(("grp", "sp"), "tp"),
            P(None, "tp", "sp"),
            P(),
            P("tp"),
        ),
        out_specs=P(("grp", "sp"), "tp"),
        check_vma=False,
    )
```

profile of v0, /device:TPU:0, one launch (start us, length us, event | category | flops | bytes accessed | tf_op | source)
XLA Modules:
  0.0 152.9 jit_solution(16187340898772377512)
XLA Ops:
  0.0 0.0 copy-start
  0.0 0.7 copy-done
  0.7 0.0 copy-start.1
  0.7 0.6 fusion.rate_ref
  1.3 0.1 copy-done.1
  1.4 0.8 reshape.20.mult_ref
  2.2 148.9 %shard_map.118 = bf16[384,512]{1,0:T(8,128)(2,1)} custom-call(bf16[384,512]{1,0:T(8,128)(2,1)} %x_ref.1, bf16[2,2,256,512]{3,2,1,0:T(8,128)(2,1)} %bitcast.4, bf16[2,2,256,512]{3,2,1,0:T(8,128)(2,1)} %bitcast.5, bf16[2,2,256,512]{3,2,1,0:T(8,128)(2,1)} %bitcast.6, bf16[2,4,512]{2,1,0:T(4,128)(2,1)} %taps_ref.1, bf16[2,2,256,256]{3,2,1,0:T(8,128)(2,1)} %reset_w.1, ...), custom_call_target="tpu_custom_call" | custom-call | tf_op jit(solution)/shard_map/pallas_call | solution.py:676
  151.1 1.8 %copy.15 = bf16[384,512]{1,0:T(8,128)(2,1)} copy(bf16[384,512]{1,0:T(8,128)(2,1)} %shard_map.118) | data formatting | bytes 786432
Async XLA Ops:
  0.0 0.7 copy-start
  0.7 0.7 copy-start.1
where the time goes:
time: 153 us
  Pallas kernels  149 us (97%)
  local copies, waits for them, and re-layouts  3.31 us (2%)
    pallas_call x1, Pallas kernels, in_one_kernel(): pl.pallas_call(functools.partial(fused, sizes), out_shape=jax.ShapeDtypeS...  149 us

commit v1 on v0

--- a/solution.py
+++ b/solution.py
@@ -143,6 +143,10 @@
 MESH = pl.DeviceIdType.MESH
 F32, BF16 = jnp.float32, jnp.bfloat16
 
+PARTS = 2
+LENT = (1,)
+WHOLE = (2, 3, 4, 5)
+
 
 def one_minus_exp(u):
     series = -u * (
@@ -186,6 +190,8 @@
     state_s,
     gel_s,
     mix_s,
+    lent_out,
+    lent_in,
     part,
     from_sib,
     pair,
@@ -193,13 +199,13 @@
     cry_out,
     cry_in,
     hacc,
+    mult_s,
     sq_out,
     sq_in,
     sem_own,
     sem_w_recv,
-    sem_up,
-    sem_down,
-    sem_y,
+    sem_w_send,
+    sem_lend,
     sem_ag_send,
     sem_ag_recv,
     sem_rs_send,
@@ -212,20 +218,21 @@
 ):
     layers, n_sp, n_tp, n_grp, rows, chans, feats, depth, pieces = sizes
     chips = n_tp // 2
+    count = 3 * layers
     g, s, t = lax.axis_index("grp"), lax.axis_index("sp"), lax.axis_index("tp")
     core = lax.rem(t, 2)
     chip = t // 2
     sib = chip * 2 + 1 - core
     full = n_tp * feats
-
-    def up():
-        return {"sp": s + 1}
-
-    def down():
-        return {"sp": s - 1}
-
-    def across():
-        return {"grp": 1 - g}
+    inw = 1 - 2 * (s // (n_sp // 2))
+    is_end = (s == 0) | (s == n_sp - 1)
+    is_mid = (s > 0) & (s < n_sp - 1)
+
+    def at_end(body):
+        pl.when(is_end)(body)
+
+    def at_mid(body):
+        pl.when(is_mid)(body)
 
     barrier = pltpu.get_barrier_semaphore()
     for d in range(1, n_tp):
@@ -236,107 +243,148 @@
         pl.semaphore_signal(
             barrier, inc=1, device_id={"sp": lax.rem(s + d, n_sp)}, device_id_type=MESH
         )
-    pl.semaphore_signal(barrier, inc=1, device_id=across(), device_id_type=MESH)
+    pl.semaphore_signal(barrier, inc=1, device_id={"grp": 1 - g}, device_id_type=MESH)
     pl.semaphore_wait(barrier, n_tp - 1 + n_sp - 1 + 1)
+
+    IN, OUT, ACROSS = 0, 1, 2
+
+    def target(way):
+        if way == ACROSS:
+            return {"grp": 1 - g}
+        return {"sp": s + inw} if way == IN else {"sp": s - inw}
 
     def own_block(m):
         return (memory_w, branch_w, exit_w)[m % 3].at[m // 3]
 
-    def held(m, j):
-        return win.at[2 * (m // 3) + m % 3, j] if m % 3 < 2 else wout.at[m // 3, j]
-
-    def sent(src, m, j, half, send_sem, where):
+    def slot(m, j):
+        kind = 2 * (m // 3) + m % 3 if m % 3 < 2 else m // 3
+        return (win if m % 3 < 2 else wout), (kind * n_sp + j) * 2
+
+    def cut(ref, q):
+        size = ref.shape[0] // PARTS
+        return ref.at[pl.ds(q * size, size)]
+
+    def held(m, j, half, q):
+        ref, at = slot(m, j)
+        return cut(ref.at[at + half], q)
+
+    def sent(src, m, j, half, q, way):
         return pltpu.make_async_remote_copy(
             src_ref=src,
-            dst_ref=held(m, j).at[half],
-            send_sem=send_sem.at[m, j],
-            recv_sem=sem_w_recv.at[m, j, half],
-            device_id=where,
+            dst_ref=held(m, j, half, q),
+            send_sem=sem_w_send.at[way],
+            recv_sem=sem_w_recv.at[m, j, half, q],
+            device_id=target(way),
             device_id_type=MESH,
         )
 
-    def start_own(m):
-        src = own_block(m).at[g]
-
-        @pl.when(s < n_sp - 1)
-        def _():
-            sent(src, m, s, g, sem_up, up()).start()
-
-        @pl.when(s > 0)
-        def _():
-            sent(src, m, s, g, sem_down, down()).start()
+    def relay(m, j, q, ways):
+        src = held(m, j, g, q)
+        for way in ways:
+            sent(src, m, j, g, q, way).start()
+
+    def landed(m, j, half, q):
+        sent(held(m, j, half, q), m, j, half, q, ACROSS).wait_recv()
+
+    def own(m, way, half):
+        for q in range(PARTS):
+            sent(cut(own_block(m).at[half], q), m, s, half, q, way).start()
+
+    def own_in(m):
+        own(m, IN, g)
+        if m in WHOLE:
+            at_end(lambda: own(m, IN, 1 - g))
 
     def keep_own(m):
-        return pltpu.make_async_copy(own_block(m), held(m, s), sem_own.at[m])
-
-    items = [(m, d) for m in range(3 * layers) for d in range(1, n_sp)]
-    place = [0]
-
-    def pump(m, d):
-        @pl.when(s - d >= 0)
-        def _():
-            j = s - d
-            src = held(m, j).at[g]
-            sent(src, m, j, g, sem_up, up()).wait_recv()
-
-            @pl.when(s < n_sp - 1)
-            def _():
-                sent(src, m, j, g, sem_up, up()).start()
-
-            sent(src, m, j, g, sem_y, across()).start()
-
-        @pl.when(s + d < n_sp)
-        def _():
-            j = s + d
-            src = held(m, j).at[g]
-            sent(src, m, j, g, sem_down, down()).wait_recv()
-
-            @pl.when(s > 0)
-            def _():
-                sent(src, m, j, g, sem_down, down()).start()
-
-            sent(src, m, j, g, sem_y, across()).start()
-
-        if d == n_sp - 1 and m + 2 < 3 * layers:
-            start_own(m + 2)
-
-    def advance(steps):
-        for m, d in items[place[0] : place[0] + steps]:
-            pump(m, d)
-        place[0] = min(place[0] + steps, len(items))
-
-    def reach(m, d):
-        advance(max(0, m * (n_sp - 1) + d - place[0]))
-
-    def swapped(m, j):
-        src = held(m, j).at[1 - g]
-        sent(src, m, j, 1 - g, sem_y, across()).wait_recv()
+        ref, at = slot(m, s)
+        return pltpu.make_async_copy(own_block(m), ref.at[pl.ds(at, 2)], sem_own.at[m])
+
+    def late():
+        return chip == (s + is_end.astype(jnp.int32) * inw) // (n_tp // chips)
+
+    def own_out(m):
+        own(m, OUT, g)
+
+    def own_out_if(m, when):
+        pl.when(is_mid & (late() if when else jnp.logical_not(late())))(lambda: own_out(m))
+
+    def end_pump(m, i):
+        if m % 3 == 2:
+            i = lax.rem(i - 1 + late().astype(jnp.int32), n_sp - 1) + 1
+        j = s + inw * i
+        for q in range(PARTS):
+            landed(m, j, g, q)
+            relay(m, j, q, (ACROSS,))
+
+    def mid_pump(m, k):
+        j = s + inw * (k if k else -1)
+        for q in range(PARTS):
+            landed(m, j, g, q)
+            if k == 0:
+                ways = (IN,) if m in WHOLE else (IN, ACROSS)
+            else:
+                ways = (ACROSS,) if m in LENT else (OUT, ACROSS)
+            relay(m, j, q, ways)
+
+    def end_do(*acts):
+        def body():
+            for act in acts:
+                act()
+
+        at_end(body)
+
+    def mid_do(*acts):
+        def body():
+            for act in acts:
+                act()
+
+        at_mid(body)
+
+    def E(m, i):
+        return lambda: end_pump(m, i)
+
+    def M(m, k):
+        return lambda: mid_pump(m, k)
+
+    def I(m):
+        return lambda: own_in(m)
+
+    def O(m):
+        return lambda: own_out(m)
+
+    def ready(m, j):
+        for q in range(PARTS):
+            landed(m, j, 1 - g, q)
 
     def arrived(m):
-        reach(m, n_sp - 1)
         keep_own(m).wait()
         for d in range(1, n_sp):
-            swapped(m, lax.rem(s + d, n_sp))
+            ready(m, lax.rem(s + d, n_sp))
+
+    def wait_sends(way, halves):
+        view = win.at[pl.ds(0, halves)]
+        pltpu.make_async_remote_copy(
+            src_ref=view,
+            dst_ref=view,
+            send_sem=sem_w_send.at[way],
+            recv_sem=sem_w_recv.at[0, 0, 0, 0],
+            device_id=target(ACROSS),
+            device_id_type=MESH,
+        ).wait_send()
 
     def close_weights():
-        for m in range(3 * layers):
-            for j in range(n_sp):
-                src = held(m, j).at[g]
-
-                @pl.when((s < n_sp - 1) & (j <= s))
-                def _():
-                    sent(src, m, j, g, sem_up, up()).wait_send()
-
-                @pl.when((s > 0) & (j >= s))
-                def _():
-                    sent(src, m, j, g, sem_down, down()).wait_send()
-
-                @pl.when(j != s)
-                def _():
-                    sent(src, m, j, g, sem_y, across()).wait_send()
-
-    for m in range(3 * layers):
-        keep_own(m).start()
+        lent, whole = len(LENT), len(WHOLE)
+
+        @at_end
+        def _():
+            wait_sends(IN, count + whole)
+            wait_sends(ACROSS, (count - lent) * (n_sp - 1))
+
+        @at_mid
+        def _():
+            wait_sends(IN, 2 * count)
+            wait_sends(OUT, (count - lent) * (n_sp - 1))
+            wait_sends(ACROSS, count * (n_sp - 1) - whole)
 
     def ag_copy(src, layer, owner, k, where):
         return pltpu.make_async_remote_copy(
@@ -370,13 +418,29 @@
             ag_copy(src, layer, t, chips + d, sib).wait_send()
         ag_copy(src, layer, t, 0, sib).wait_send()
 
-    ag_start(0, x_ref)
-    for m in range(2):
-        start_own(m)
+    def lend_rows():
+        return pltpu.make_async_remote_copy(
+            src_ref=x_ref,
+            dst_ref=agx.at[layers, t],
+            send_sem=sem_lend.at[0],
+            recv_sem=sem_ag_recv.at[layers, t],
+            device_id=target(IN),
+            device_id_type=MESH,
+        )
+
+    def lend_back():
+        return pltpu.make_async_remote_copy(
+            src_ref=lent_out,
+            dst_ref=lent_in,
+            send_sem=sem_lend.at[1],
+            recv_sem=sem_lend.at[2],
+            device_id=target(OUT),
+            device_id_type=MESH,
+        )
 
     step = rows // pieces
 
-    def normalize(layer):
+    def normalize(layer, gain_row):
         def one(i, carry):
             at = pl.ds(pl.multiple_of(i * step, step), step)
             total = jnp.zeros((step, 1), F32)
@@ -387,7 +451,7 @@
             for p in range(n_tp):
                 cols = slice(p * feats, (p + 1) * feats)
                 f = agx[layer, p, at].astype(F32)
-                gain = gains_ref[layer : layer + 1, cols]
+                gain = gains_ref[gain_row : gain_row + 1, cols]
                 nrm[at, cols] = (f * inv * gain).astype(BF16)
             return carry
 
@@ -396,13 +460,14 @@
     def project(idx):
         total = None
         for j in range(n_sp):
+            at = (idx * n_sp + j) * 2
             term = jnp.dot(
                 nrm[:, j * depth : (j + 1) * depth],
-                win[idx, j].reshape(depth, chans),
+                win[at : at + 2].reshape(depth, chans),
                 preferred_element_type=F32,
             )
             total = term if total is None else total + term
-        return total.astype(BF16).astype(F32)
+        return total.astype(BF16)
 
     def halo_copy(layer):
         return pltpu.make_async_remote_copy(
@@ -410,7 +475,7 @@
             dst_ref=halo.at[layer],
             send_sem=sem_h.at[layer, 0],
             recv_sem=sem_h.at[layer, 1],
-            device_id=up(),
+            device_id={"sp": s + 1},
             device_id_type=MESH,
         )
 
@@ -452,24 +517,12 @@
         where = lax.rem(t + 2 * q, n_tp)
         return rs_copy(pair.at[layer, q], from_far.at[layer, q], layer, chips + q, where)
 
-    for layer in range(layers):
-        m0 = 3 * layer
-        src = x_ref if layer == 0 else xs.at[layer]
-        agx[layer, t] = src[...]
-        advance(1)
-        ag_finish(layer, src)
-        advance(1)
-        normalize(layer)
-        reach(m0, n_sp)
-        arrived(m0)
-        ext[layer, 8:] = project(2 * layer)
-
+    def send_halo(layer):
         @pl.when(s < n_sp - 1)
         def _():
             halo_copy(layer).start()
 
-        advance(1)
-
+    def take_halo(layer):
         @pl.when(s == 0)
         def _():
             halo[layer] = jnp.zeros((8, chans), F32)
@@ -479,46 +532,45 @@
             halo_copy(layer).wait_recv()
 
         ext[layer, :8] = halo[layer]
+
+    def gates(layer, b):
         n_taps = taps_ref.shape[1]
         base = 8 - (n_taps - 1)
-        for b in range(chans // BLOCK_W):
-            cols = slice(b * BLOCK_W, (b + 1) * BLOCK_W)
-            conv = jnp.zeros((rows, BLOCK_W), F32)
-            for k in range(n_taps):
-                tap = taps_ref[layer, k : k + 1, cols].astype(F32)
-                conv = conv + ext[layer, base + k : base + k + rows, cols] * tap
-            conv = conv.astype(BF16)
-            reset = jax.nn.sigmoid(
-                jnp.dot(conv, reset_w[layer, b], preferred_element_type=F32)
-            )
-            inject = jax.nn.sigmoid(
-                jnp.dot(conv, inject_w[layer, b], preferred_element_type=F32)
-            )
-            log_keep = (
-                reset * rate_ref[layer : layer + 1, cols] * mult_ref[...]
-                + spike_ref[:, cols]
-            )
-            keep = jnp.exp(log_keep)
-            state = inject * conv.astype(F32) * jnp.sqrt(one_minus_exp(2.0 * log_keep))
-            lag = 1
-            while lag < rows:
-                state = keep * shifted(state, lag, 0.0) + state
-                keep = keep * shifted(keep, lag, 1.0)
-                lag *= 2
-            keep_s[:, cols] = keep
-            state_s[:, cols] = state
-            cry_out[layer, 0:1, cols] = keep[rows - 1 :]
-            cry_out[layer, 1:2, cols] = state[rows - 1 :]
-            advance(1)
+        cols = slice(b * BLOCK_W, (b + 1) * BLOCK_W)
+        conv = jnp.zeros((rows, BLOCK_W), F32)
+        for k in range(n_taps):
+            tap = taps_ref[layer, k : k + 1, cols].astype(F32)
+            conv = conv + ext[layer, base + k : base + k + rows, cols] * tap
+        conv = conv.astype(BF16)
+        reset = jax.nn.sigmoid(
+            jnp.dot(conv, reset_w[layer, b], preferred_element_type=F32)
+        )
+        inject = jax.nn.sigmoid(
+            jnp.dot(conv, inject_w[layer, b], preferred_element_type=F32)
+        )
+        log_keep = (
+            reset * rate_ref[layer : layer + 1, cols] * mult_s[...] + spike_ref[:, cols]
+        )
+        keep = jnp.exp(log_keep)
+        state = inject * conv.astype(F32) * jnp.sqrt(one_minus_exp(2.0 * log_keep))
+        lag = 1
+        while lag < rows:
+            state = keep * shifted(state, lag, 0.0) + state
+            keep = keep * shifted(keep, lag, 1.0)
+            lag *= 2
+        keep_s[:, cols] = keep
+        state_s[:, cols] = state
+        cry_out[layer, 0:1, cols] = keep[rows - 1 :]
+        cry_out[layer, 1:2, cols] = state[rows - 1 :]
+
+    def send_carry(layer):
         for d in range(1, n_sp):
 
             @pl.when(s + d < n_sp)
             def _():
                 carry_copy(layer, d).start()
 
-        reach(m0 + 2, min(2, n_sp - 1))
-        arrived(m0 + 1)
-        gel_s[...] = jax.nn.gelu(project(2 * layer + 1))
+    def take_carry(layer):
         hacc[...] = jnp.zeros((1, chans), F32)
         for j in range(n_sp - 1):
 
@@ -527,68 +579,59 @@
                 carry_wait(layer, j)
                 hacc[...] = cry_in[layer, j, 0:1] * hacc[...] + cry_in[layer, j, 1:2]
 
+    def mix():
         mix_s[...] = (
             gel_s[...] * (state_s[...] + keep_s[...] * hacc[...])
         ).astype(BF16)
-        def chips_on(j):
-            return lax.rem(j // 2 - chip + chips, chips)
-
-        def product(j):
-            part[layer, j] = jnp.dot(
-                mix_s[...],
-                wout[layer, j].reshape(chans, depth),
-                preferred_element_type=F32,
+
+    def chips_on(j):
+        return lax.rem(j // 2 - chip + chips, chips)
+
+    def product(layer, j):
+        at = (layer * n_sp + j) * 2
+        part[layer, j] = jnp.dot(
+            mix_s[...],
+            wout[pl.ds(at, 2)].reshape(chans, depth),
+            preferred_element_type=F32,
+        ).astype(BF16)
+
+        @pl.when(lax.rem(j, 2) != core)
+        def _():
+            near_copy(layer, chips_on(j)).start()
+
+    def pass_on(layer, j):
+        q = chips_on(j)
+
+        @pl.when((lax.rem(j, 2) == core) & (q != 0))
+        def _():
+            near_copy(layer, q).wait_recv()
+            pair[layer, q] = (
+                part[layer, j].astype(F32) + from_sib[layer, q].astype(F32)
             ).astype(BF16)
-
-            @pl.when(lax.rem(j, 2) != core)
-            def _():
-                near_copy(layer, chips_on(j)).start()
-
-        def pass_on(j):
-            q = chips_on(j)
-
-            @pl.when((lax.rem(j, 2) == core) & (q != 0))
-            def _():
-                near_copy(layer, q).wait_recv()
-                pair[layer, q] = (
-                    part[layer, j].astype(F32) + from_sib[layer, q].astype(F32)
-                ).astype(BF16)
-                far_copy(layer, q).start()
-
-        m = m0 + 2
+            far_copy(layer, q).start()
+
+    def exit_order(i):
+        turned = lax.rem(i - 1 + late().astype(jnp.int32), n_sp - 1) + 1
+        end_step = turned
+        mid_step = (-1, 1, 2)[i - 1]
+        e = is_end.astype(jnp.int32)
+        return s + inw * (e * end_step + (1 - e) * mid_step)
+
+    def project_out(layer, ahead):
+        m = 3 * layer + 2
         keep_own(m).wait()
-        product(s)
-        for d in range(1, n_sp):
-            reach(m, d)
-            if d > 1:
-                advance(1)
-
-            @pl.when(s - d >= 0)
-            def _():
-                swapped(m, s - d)
-                product(s - d)
-
-            @pl.when(s + d < n_sp)
-            def _():
-                swapped(m, s + d)
-                product(s + d)
-
-            if d == 1:
-                pass_on(s)
-            else:
-                for j in (s - d + 1, s + d - 1):
-
-                    @pl.when((j >= 0) & (j < n_sp))
-                    def _():
-                        pass_on(j)
-
-        for j in (s - n_sp + 1, s + n_sp - 1):
-
-            @pl.when((j >= 0) & (j < n_sp))
-            def _():
-                pass_on(j)
-
-        advance(1)
+        product(layer, s)
+        before = s
+        for i in range(1, n_sp):
+            ahead(i)
+            j = exit_order(i)
+            ready(m, j)
+            product(layer, j)
+            pass_on(layer, before)
+            before = j
+        pass_on(layer, before)
+
+    def close_layer(layer, src):
         near_copy(layer, 0).wait_recv()
         mixed = part[layer, t].astype(F32) + from_sib[layer, 0].astype(F32)
         for q in range(1, chips):
@@ -596,11 +639,104 @@
             mixed = mixed + from_far[layer, q].astype(F32)
         fresh = (src[...].astype(F32) + mixed).astype(BF16)
         xs[layer + 1] = fresh
-        if layer + 1 < layers:
-            ag_start(layer + 1, xs.at[layer + 1])
-
-    last = xs[layers].astype(F32)
-    square = jnp.sum(last * last, axis=1, keepdims=True)
+
+    ag_start(0, x_ref)
+    own_in(0)
+    at_end(lambda: lend_rows().start())
+    own_in(1)
+    mid_do(O(0), O(3))
+    for m in range(count):
+        keep_own(m).start()
+    agx[0, t] = x_ref[...]
+    mult_s[...] = jnp.broadcast_to(mult_ref[...], (128, rows)).T[:, 0:1]
+
+    end_do(E(0, 1), I(2))
+    mid_do(M(0, 0), M(0, 1))
+    ag_finish(0, x_ref)
+    normalize(0, 0)
+
+    @at_mid
+    def _():
+        lend_rows().wait_recv()
+        ag_start(layers, agx.at[layers, t])
+
+    mid_do(M(0, 2), I(2), M(1, 1))
+    end_do(E(3, 1), E(0, 2), E(0, 3), I(3))
+    arrived(0)
+    ext[0, 8:] = project(0).astype(F32)
+    send_halo(0)
+    mid_do(M(1, 0), O(4))
+    take_halo(0)
+    gates(0, 0)
+    mid_do(M(1, 2), I(3))
+    gates(0, 1)
+    send_carry(0)
+    end_do(E(4, 1), I(4))
+
+    @at_mid
+    def _():
+        arrived(1)
+        gel_s[...] = jax.nn.gelu(project(1).astype(F32))
+        ag_finish(layers, agx.at[layers, t])
+        normalize(layers, 0)
+        lent_out[...] = project(1)
+        lend_back().start()
+        own_out_if(2, False)
+
+    mid_do(M(2, 0), M(2, 1))
+
+    @at_end
+    def _():
+        keep_own(1).wait()
+        lend_back().wait_recv()
+        gel_s[...] = jax.nn.gelu(lent_in[...].astype(F32))
+
+    take_carry(0)
+    mix()
+
+    def ahead(i):
+        if i == 1:
+            end_do(E(2, 1), I(5))
+        elif i == 2:
+            end_do(E(2, 2))
+        else:
+            end_do(E(2, 3))
+            mid_do(M(2, 2), lambda: own_out_if(2, True), I(4), M(3, 1), M(3, 0))
+
+    project_out(0, ahead)
+    close_layer(0, x_ref)
+
+    ag_start(1, xs.at[1])
+    agx[1, t] = xs[1]
+    mid_do(M(3, 2), I(5))
+    end_do(E(3, 2), E(3, 3))
+    ag_finish(1, xs.at[1])
+    normalize(1, 1)
+    arrived(3)
+    ext[1, 8:] = project(2).astype(F32)
+    send_halo(1)
+    mid_do(M(4, 1), M(4, 0))
+    take_halo(1)
+    gates(1, 0)
+    mid_do(M(4, 2), lambda: own_out_if(5, False))
+    end_do(E(4, 2))
+    gates(1, 1)
+    send_carry(1)
+    mid_do(M(5, 1), M(5, 0), M(5, 2), lambda: own_out_if(5, True))
+    end_do(E(4, 3))
+    arrived(4)
+    gel_s[...] = jax.nn.gelu(project(3).astype(F32))
+    take_carry(1)
+    mix()
+
+    def ahead_last(i):
+        end_do(E(5, i))
+
+    project_out(1, ahead_last)
+    close_layer(1, xs.at[1])
+
+    fresh = xs[layers].astype(F32)
+    square = jnp.sum(fresh * fresh, axis=1, keepdims=True)
     sq_out[...] = jnp.broadcast_to(square, (rows, 128)).T[0:8]
 
     def sq_copy(d):
@@ -624,6 +760,13 @@
     out_ref[...] = (xs[layers].astype(F32) * inv * final_ref[...]).astype(BF16)
 
     close_weights()
+    at_end(lambda: lend_rows().wait_send())
+
+    @at_mid
+    def _():
+        ag_close(layers, agx.at[layers, t])
+        lend_back().wait_send()
+
     for layer in range(layers):
         ag_close(layer, x_ref if layer == 0 else xs.at[layer])
 
@@ -679,9 +822,9 @@
         in_specs=[vmem, hbm, hbm, hbm] + [vmem] * 8,
         out_specs=vmem,
         scratch_shapes=[
-            pltpu.VMEM((2 * layers, n_sp, 2, depth // 2, chans), BF16),
-            pltpu.VMEM((layers, n_sp, 2, chans // 2, depth), BF16),
-            pltpu.VMEM((layers, n_tp, rows, feats), BF16),
+            pltpu.VMEM((2 * layers * n_sp * 2, depth // 2, chans), BF16),
+            pltpu.VMEM((layers * n_sp * 2, chans // 2, depth), BF16),
+            pltpu.VMEM((layers + 1, n_tp, rows, feats), BF16),
             pltpu.VMEM((layers + 1, rows, feats), BF16),
             pltpu.VMEM((rows, n_tp * feats), BF16),
             pltpu.VMEM((layers, 8 + rows, chans), F32),
@@ -690,6 +833,8 @@
             pltpu.VMEM((rows, chans), F32),
             pltpu.VMEM((rows, chans), F32),
             pltpu.VMEM((rows, chans), BF16),
+            pltpu.VMEM((rows, chans), BF16),
+            pltpu.VMEM((rows, chans), BF16),
             pltpu.VMEM((layers, n_tp, rows, feats), BF16),
             pltpu.VMEM((layers, chips, rows, feats), BF16),
             pltpu.VMEM((layers, chips, rows, feats), BF16),
@@ -697,15 +842,15 @@
             pltpu.VMEM((layers, 2, chans), F32),
             pltpu.VMEM((layers, n_sp, 2, chans), F32),
             pltpu.VMEM((1, chans), F32),
+            pltpu.VMEM((rows, 1), F32),
             pltpu.VMEM((8, rows), F32),
             pltpu.VMEM((n_tp, 8, rows), F32),
             dma((count,)),
-            dma((count, n_sp, 2)),
-            dma((count, n_sp)),
-            dma((count, n_sp)),
-            dma((count, n_sp)),
-            dma((layers, 2 * chips)),
-            dma((layers, n_tp)),
+            dma((count, n_sp, 2, PARTS)),
+            dma((3,)),
+            dma((3,)),
+            dma((layers + 1, 2 * chips)),
+            dma((layers + 1, n_tp)),
             dma((layers, 2 * chips)),
             dma((layers, 2 * chips)),
             dma((layers, 2)),
@@ -726,7 +871,7 @@
         memory_valve_matrix,
         entry_valve_matrix,
         rate,
-        timestep_forgetting_multiplier.reshape(rows, 1),
+        timestep_forgetting_multiplier.reshape(1, rows),
         spike_extra,
         prelude_rms_gains,
         finishing_rms_gains.reshape(1, feats),
@@ -740,7 +885,8 @@
     depth, chans = memory.shape[1:]
     fits = (
         n_grp == 2
-        and n_sp > 1
+        and n_sp == 4
+        and memory.shape[0] == 2
         and n_tp % 2 == 0
         and rows % 128 == 0
         and depth % 128 == 0

time: 153 us -> 171 us (1.12)
  Pallas kernels: 149 us -> 167 us
    pallas_call x1, Pallas kernels: 149 us -> 167 us  [in_one_kernel(): pl.pallas_call(functools.partial(fused, sizes), out_shape=jax.ShapeDtypeS...]
where the time goes in v1:
time: 171 us
  Pallas kernels  167 us (98%)
  local copies, waits for them, and re-layouts  3.04 us (2%)
    pallas_call x1, Pallas kernels, in_one_kernel(): pl.pallas_call(functools.partial(fused, sizes), out_shape=jax.ShapeDtypeS...  167 us

profile of v1, /device:TPU:0, one launch (start us, length us, event | category | flops | bytes accessed | tf_op | source)
XLA Modules:
  0.0 170.6 jit_solution(17333126622971095464)
XLA Ops:
  0.0 0.0 copy-start.1
  0.0 0.0 copy-start
  0.0 0.7 copy-done.1
  0.7 0.6 reshape.18.mult_ref
  1.3 0.0 copy-done
  1.3 0.6 fusion.rate_ref
  1.9 166.9 %shard_map.118 = bf16[384,512]{1,0:T(8,128)(2,1)} custom-call(bf16[384,512]{1,0:T(8,128)(2,1)} %x_ref.1, bf16[2,2,256,512]{3,2,1,0:T(8,128)(2,1)} %bitcast.4, bf16[2,2,256,512]{3,2,1,0:T(8,128)(2,1)} %bitcast.5, bf16[2,2,256,512]{3,2,1,0:T(8,128)(2,1)} %bitcast.6, bf16[2,4,512]{2,1,0:T(4,128)(2,1)} %taps_ref.1, bf16[2,2,256,256]{3,2,1,0:T(8,128)(2,1)} %reset_w.1, ...), custom_call_target="tpu_custom_call" | custom-call | tf_op jit(solution)/shard_map/pallas_call | solution.py:819
  168.8 1.8 %copy.14 = bf16[384,512]{1,0:T(8,128)(2,1)} copy(bf16[384,512]{1,0:T(8,128)(2,1)} %shard_map.118) | data formatting | bytes 786432
Async XLA Ops:
  0.0 0.7 copy-start.1
  0.0 1.3 copy-start

commit v2 on v1

--- a/solution.py
+++ b/solution.py
@@ -143,9 +143,10 @@
 MESH = pl.DeviceIdType.MESH
 F32, BF16 = jnp.float32, jnp.bfloat16
 
-PARTS = 2
-LENT = (1,)
-WHOLE = (2, 3, 4, 5)
+PARTS = 4
+BANDS = 2
+LENT = (0, 1)
+WHOLE = (1, 2, 3, 4, 5)
 
 
 def one_minus_exp(u):
@@ -184,6 +185,7 @@
     agx,
     xs,
     nrm,
+    nrm_lent,
     ext,
     halo,
     keep_s,
@@ -286,14 +288,29 @@
     def landed(m, j, half, q):
         sent(held(m, j, half, q), m, j, half, q, ACROSS).wait_recv()
 
-    def own(m, way, half):
+    def own(m, way, half, q):
+        sent(cut(own_block(m).at[half], q), m, s, half, q, way).start()
+
+    def own_both(m, way):
         for q in range(PARTS):
-            sent(cut(own_block(m).at[half], q), m, s, half, q, way).start()
-
-    def own_in(m):
-        own(m, IN, g)
-        if m in WHOLE:
-            at_end(lambda: own(m, IN, 1 - g))
+            own(m, way, g, q)
+
+    halves = [(1, g)]
+    for m in range(2, count):
+        halves += [(m, g), (m - 1, 1 - g)]
+    halves.append((count - 1, 1 - g))
+    end_line = [(m, half, q) for m, half in halves for q in range(PARTS)]
+    mid_in_line = [(m, q) for m in range(1, count) for q in range(PARTS)]
+    def feed_end(steps):
+        steps *= PARTS // 2
+        for m, half, q in end_line[:steps]:
+            own(m, IN, half, q)
+        del end_line[:steps]
+
+    def feed_in(steps):
+        for m, q in mid_in_line[:steps]:
+            own(m, IN, g, q)
+        del mid_in_line[:steps]
 
     def keep_own(m):
         ref, at = slot(m, s)
@@ -302,21 +319,23 @@
     def late():
         return chip == (s + is_end.astype(jnp.int32) * inw) // (n_tp // chips)
 
-    def own_out(m):
-        own(m, OUT, g)
+    def end_turn(i):
+        return lax.rem(i - 1 + late().astype(jnp.int32), n_sp - 1) + 1
 
     def own_out_if(m, when):
-        pl.when(is_mid & (late() if when else jnp.logical_not(late())))(lambda: own_out(m))
-
-    def end_pump(m, i):
-        if m % 3 == 2:
-            i = lax.rem(i - 1 + late().astype(jnp.int32), n_sp - 1) + 1
-        j = s + inw * i
+        @pl.when(late() if when else jnp.logical_not(late()))
+        def _():
+            own_both(m, OUT)
+
+    def end_pump(m, i, feed):
+        j = s + inw * (end_turn(i) if m == count - 1 else i)
         for q in range(PARTS):
             landed(m, j, g, q)
             relay(m, j, q, (ACROSS,))
-
-    def mid_pump(m, k):
+            if q % (PARTS // 2) == PARTS // 2 - 1:
+                feed_end(feed)
+
+    def mid_pump(m, k, feed):
         j = s + inw * (k if k else -1)
         for q in range(PARTS):
             landed(m, j, g, q)
@@ -325,6 +344,7 @@
             else:
                 ways = (ACROSS,) if m in LENT else (OUT, ACROSS)
             relay(m, j, q, ways)
+        feed_in(feed)
 
     def end_do(*acts):
         def body():
@@ -340,17 +360,14 @@
 
         at_mid(body)
 
-    def E(m, i):
-        return lambda: end_pump(m, i)
-
-    def M(m, k):
-        return lambda: mid_pump(m, k)
-
-    def I(m):
-        return lambda: own_in(m)
-
-    def O(m):
-        return lambda: own_out(m)
+    def E(m, i, feed=0):
+        return lambda: end_pump(m, i, feed)
+
+    def M(m, k, feed=0):
+        return lambda: mid_pump(m, k, feed)
+
+    def F(steps):
+        return lambda: feed_end(steps)
 
     def ready(m, j):
         for q in range(PARTS):
@@ -386,61 +403,67 @@
             wait_sends(OUT, (count - lent) * (n_sp - 1))
             wait_sends(ACROSS, count * (n_sp - 1) - whole)
 
-    def ag_copy(src, layer, owner, k, where):
+    def band(ref, h):
+        return ref.at[pl.ds(h * (rows // BANDS), rows // BANDS)]
+
+    def ag_copy(src, layer, owner, k, h, where):
         return pltpu.make_async_remote_copy(
-            src_ref=src,
-            dst_ref=agx.at[layer, owner],
-            send_sem=sem_ag_send.at[layer, k],
-            recv_sem=sem_ag_recv.at[layer, owner],
+            src_ref=band(src, h),
+            dst_ref=band(agx.at[layer, owner], h),
+            send_sem=sem_ag_send.at[layer, k, h],
+            recv_sem=sem_ag_recv.at[layer, owner, h],
             device_id={"tp": where},
             device_id_type=MESH,
         )
 
-    def ag_start(layer, src):
+    def ag_start(layer, src, h):
         for d in range(1, chips):
-            ag_copy(src, layer, t, d, lax.rem(t + 2 * d, n_tp)).start()
-        ag_copy(src, layer, t, 0, sib).start()
+            ag_copy(src, layer, t, d, h, lax.rem(t + 2 * d, n_tp)).start()
+        ag_copy(src, layer, t, 0, h, sib).start()
 
     def ag_finish(layer, src):
-        for d in range(1, chips):
-            owner = lax.rem(t + 2 * d, n_tp)
-            block = agx.at[layer, owner]
-            ag_copy(block, layer, owner, d, sib).wait_recv()
-            ag_copy(block, layer, owner, chips + d, sib).start()
-        ag_copy(src, layer, sib, 0, sib).wait_recv()
-        for d in range(1, chips):
-            owner = lax.rem(sib + 2 * d, n_tp)
-            ag_copy(agx.at[layer, owner], layer, owner, d, sib).wait_recv()
+        for h in range(BANDS):
+            for d in range(1, chips):
+                owner = lax.rem(t + 2 * d, n_tp)
+                block = agx.at[layer, owner]
+                ag_copy(block, layer, owner, d, h, sib).wait_recv()
+                ag_copy(block, layer, owner, chips + d, h, sib).start()
+        for h in range(BANDS):
+            ag_copy(src, layer, sib, 0, h, sib).wait_recv()
+            for d in range(1, chips):
+                owner = lax.rem(sib + 2 * d, n_tp)
+                ag_copy(agx.at[layer, owner], layer, owner, d, h, sib).wait_recv()
 
     def ag_close(layer, src):
-        for d in range(1, chips):
-            ag_copy(src, layer, t, d, sib).wait_send()
-            ag_copy(src, layer, t, chips + d, sib).wait_send()
-        ag_copy(src, layer, t, 0, sib).wait_send()
-
-    def lend_rows():
+        for h in range(BANDS):
+            for d in range(1, chips):
+                ag_copy(src, layer, t, d, h, sib).wait_send()
+                ag_copy(src, layer, t, chips + d, h, sib).wait_send()
+            ag_copy(src, layer, t, 0, h, sib).wait_send()
+
+    def lend_rows(h):
         return pltpu.make_async_remote_copy(
-            src_ref=x_ref,
-            dst_ref=agx.at[layers, t],
-            send_sem=sem_lend.at[0],
-            recv_sem=sem_ag_recv.at[layers, t],
+            src_ref=band(x_ref, h),
+            dst_ref=band(agx.at[layers, t], h),
+            send_sem=sem_lend.at[h],
+            recv_sem=sem_ag_recv.at[layers, t, h],
             device_id=target(IN),
             device_id_type=MESH,
         )
 
-    def lend_back():
+    def lend_back(i):
         return pltpu.make_async_remote_copy(
-            src_ref=lent_out,
-            dst_ref=lent_in,
-            send_sem=sem_lend.at[1],
-            recv_sem=sem_lend.at[2],
+            src_ref=lent_out.at[i],
+            dst_ref=lent_in.at[i],
+            send_sem=sem_lend.at[BANDS + i],
+            recv_sem=sem_lend.at[BANDS + len(LENT) + i],
             device_id=target(OUT),
             device_id_type=MESH,
         )
 
     step = rows // pieces
 
-    def normalize(layer, gain_row):
+    def normalize(layer, gain_row, nrm):
         def one(i, carry):
             at = pl.ds(pl.multiple_of(i * step, step), step)
             total = jnp.zeros((step, 1), F32)
@@ -457,7 +480,7 @@
 
         lax.fori_loop(0, pieces, one, 0)
 
-    def project(idx):
+    def project(idx, nrm):
         total = None
         for j in range(n_sp):
             at = (idx * n_sp + j) * 2
@@ -499,26 +522,31 @@
             device_id_type=MESH,
         ).wait_recv()
 
-    def rs_copy(src, dst, layer, k, where):
+    def rs_copy(src, dst, layer, k, h, where):
         return pltpu.make_async_remote_copy(
             src_ref=src,
             dst_ref=dst,
-            send_sem=sem_rs_send.at[layer, k],
-            recv_sem=sem_rs_recv.at[layer, k],
+            send_sem=sem_rs_send.at[layer, k, h],
+            recv_sem=sem_rs_recv.at[layer, k, h],
             device_id={"tp": where},
             device_id_type=MESH,
         )
 
-    def near_copy(layer, q):
+    def near_copy(layer, q, h):
         to = lax.rem(sib + 2 * q, n_tp)
-        return rs_copy(part.at[layer, to], from_sib.at[layer, q], layer, q, sib)
-
-    def far_copy(layer, q):
+        src, dst = band(part.at[layer, to], h), band(from_sib.at[layer, q], h)
+        return rs_copy(src, dst, layer, q, h, sib)
+
+    def far_copy(layer, q, h):
         where = lax.rem(t + 2 * q, n_tp)
-        return rs_copy(pair.at[layer, q], from_far.at[layer, q], layer, chips + q, where)
+        src, dst = band(pair.at[layer, q], h), band(from_far.at[layer, q], h)
+        return rs_copy(src, dst, layer, chips + q, h, where)
+
+    def first_sender(layer):
+        return 1 if layer == 0 else 0
 
     def send_halo(layer):
-        @pl.when(s < n_sp - 1)
+        @pl.when((s >= first_sender(layer)) & (s < n_sp - 1))
         def _():
             halo_copy(layer).start()
 
@@ -527,7 +555,13 @@
         def _():
             halo[layer] = jnp.zeros((8, chans), F32)
 
-        @pl.when(s > 0)
+        if layer == 0:
+
+            @pl.when(s == 1)
+            def _():
+                halo[layer] = lent_out[0].astype(F32)[rows - 8 :]
+
+        @pl.when(s > first_sender(layer))
         def _():
             halo_copy(layer).wait_recv()
 
@@ -597,22 +631,24 @@
 
         @pl.when(lax.rem(j, 2) != core)
         def _():
-            near_copy(layer, chips_on(j)).start()
+            for h in range(BANDS):
+                near_copy(layer, chips_on(j), h).start()
 
     def pass_on(layer, j):
         q = chips_on(j)
 
         @pl.when((lax.rem(j, 2) == core) & (q != 0))
         def _():
-            near_copy(layer, q).wait_recv()
-            pair[layer, q] = (
-                part[layer, j].astype(F32) + from_sib[layer, q].astype(F32)
-            ).astype(BF16)
-            far_copy(layer, q).start()
-
-    def exit_order(i):
-        turned = lax.rem(i - 1 + late().astype(jnp.int32), n_sp - 1) + 1
-        end_step = turned
+            for h in range(BANDS):
+                at = pl.ds(h * (rows // BANDS), rows // BANDS)
+                near_copy(layer, q, h).wait_recv()
+                pair[layer, q, at] = (
+                    part[layer, j, at].astype(F32) + from_sib[layer, q, at].astype(F32)
+                ).astype(BF16)
+                far_copy(layer, q, h).start()
+
+    def exit_order(layer, i):
+        end_step = end_turn(i) if layer == layers - 1 else i
         mid_step = (-1, 1, 2)[i - 1]
         e = is_end.astype(jnp.int32)
         return s + inw * (e * end_step + (1 - e) * mid_step)
@@ -624,7 +660,7 @@
         before = s
         for i in range(1, n_sp):
             ahead(i)
-            j = exit_order(i)
+            j = exit_order(layer, i)
             ready(m, j)
             product(layer, j)
             pass_on(layer, before)
@@ -632,105 +668,133 @@
         pass_on(layer, before)
 
     def close_layer(layer, src):
-        near_copy(layer, 0).wait_recv()
-        mixed = part[layer, t].astype(F32) + from_sib[layer, 0].astype(F32)
-        for q in range(1, chips):
-            far_copy(layer, q).wait_recv()
-            mixed = mixed + from_far[layer, q].astype(F32)
-        fresh = (src[...].astype(F32) + mixed).astype(BF16)
-        xs[layer + 1] = fresh
-
-    ag_start(0, x_ref)
-    own_in(0)
-    at_end(lambda: lend_rows().start())
-    own_in(1)
-    mid_do(O(0), O(3))
-    for m in range(count):
-        keep_own(m).start()
-    agx[0, t] = x_ref[...]
-    mult_s[...] = jnp.broadcast_to(mult_ref[...], (128, rows)).T[:, 0:1]
-
-    end_do(E(0, 1), I(2))
-    mid_do(M(0, 0), M(0, 1))
-    ag_finish(0, x_ref)
-    normalize(0, 0)
+        for h in range(BANDS):
+            at = pl.ds(h * (rows // BANDS), rows // BANDS)
+            near_copy(layer, 0, h).wait_recv()
+            mixed = part[layer, t, at].astype(F32) + from_sib[layer, 0, at].astype(F32)
+            for q in range(1, chips):
+                far_copy(layer, q, h).wait_recv()
+                mixed = mixed + from_far[layer, q, at].astype(F32)
+            xs[layer + 1, at] = (src[at].astype(F32) + mixed).astype(BF16)
+            if layer + 1 < layers:
+                ag_start(layer + 1, xs.at[layer + 1], h)
+
+    own_both(0, IN)
+
+    @at_end
+    def _():
+        for h in range(BANDS):
+            lend_rows(h).start()
+        feed_end(2)
 
     @at_mid
     def _():
-        lend_rows().wait_recv()
-        ag_start(layers, agx.at[layers, t])
-
-    mid_do(M(0, 2), I(2), M(1, 1))
-    end_do(E(3, 1), E(0, 2), E(0, 3), I(3))
-    arrived(0)
-    ext[0, 8:] = project(0).astype(F32)
-    send_halo(0)
-    mid_do(M(1, 0), O(4))
+        for h in range(BANDS):
+            ag_start(0, x_ref, h)
+        for m in (2, 3, 4):
+            own_both(m, OUT)
+        for m in LENT:
+            keep_own(m).start()
+        agx[0, t] = x_ref[...]
+
+    for m in range(len(LENT), count):
+        keep_own(m).start()
+    mult_s[...] = jnp.broadcast_to(mult_ref[...], (128, rows)).T[:, 0:1]
+
+    @at_mid
+    def _():
+        mid_pump(0, 0, PARTS)
+        mid_pump(0, 1, 0)
+        ag_finish(0, x_ref)
+        normalize(0, 0, nrm)
+        lend_rows(0).wait_recv()
+        ag_start(layers, agx.at[layers, t], 0)
+        mid_pump(0, 2, PARTS)
+        for h in range(1, BANDS):
+            lend_rows(h).wait_recv()
+            ag_start(layers, agx.at[layers, t], h)
+        mid_pump(1, 1, 0)
+        mid_pump(1, 0, 0)
+        arrived(0)
+        ext[0, 8:] = project(0, nrm).astype(F32)
+        send_halo(0)
+        mid_pump(2, 1, 0)
+        ag_finish(layers, agx.at[layers, t])
+        normalize(layers, 0, nrm_lent)
+        lent_out[0] = project(0, nrm_lent)
+        lend_back(0).start()
+        mid_pump(2, 0, PARTS)
+        mid_pump(1, 2, 0)
+
+    @at_end
+    def _():
+        end_pump(2, 1, 0)
+        end_pump(3, 1, 0)
+        end_pump(4, 1, 1)
+        feed_end(2)
+        end_pump(2, 2, 1)
+        feed_end(2)
+        lend_back(0).wait_recv()
+        ext[0, 8:] = lent_in[0].astype(F32)
+
     take_halo(0)
     gates(0, 0)
-    mid_do(M(1, 2), I(3))
     gates(0, 1)
     send_carry(0)
-    end_do(E(4, 1), I(4))
 
     @at_mid
     def _():
+        mid_pump(2, 2, 0)
         arrived(1)
-        gel_s[...] = jax.nn.gelu(project(1).astype(F32))
-        ag_finish(layers, agx.at[layers, t])
-        normalize(layers, 0)
-        lent_out[...] = project(1)
-        lend_back().start()
-        own_out_if(2, False)
-
-    mid_do(M(2, 0), M(2, 1))
+        lent_out[1] = project(1, nrm_lent)
+        lend_back(1).start()
+        gel_s[...] = jax.nn.gelu(project(1, nrm).astype(F32))
+        mid_pump(3, 1, 0)
+        mid_pump(3, 0, PARTS)
 
     @at_end
     def _():
-        keep_own(1).wait()
-        lend_back().wait_recv()
-        gel_s[...] = jax.nn.gelu(lent_in[...].astype(F32))
+        feed_end(4)
+        end_pump(2, 3, 0)
+        lend_back(1).wait_recv()
+        feed_end(2)
+        gel_s[...] = jax.nn.gelu(lent_in[1].astype(F32))
 
     take_carry(0)
     mix()
 
     def ahead(i):
-        if i == 1:
-            end_do(E(2, 1), I(5))
-        elif i == 2:
-            end_do(E(2, 2))
-        else:
-            end_do(E(2, 3))
-            mid_do(M(2, 2), lambda: own_out_if(2, True), I(4), M(3, 1), M(3, 0))
+        if i == 3:
+            mid_do(M(3, 2), M(4, 1))
 
     project_out(0, ahead)
+    mid_do(M(4, 0, PARTS))
+    end_do(F(2))
     close_layer(0, x_ref)
 
-    ag_start(1, xs.at[1])
     agx[1, t] = xs[1]
-    mid_do(M(3, 2), I(5))
-    end_do(E(3, 2), E(3, 3))
+    mid_do(M(4, 2), lambda: own_out_if(5, False), M(5, 1))
+    end_do(E(3, 2, 1), E(3, 3), F(99), E(4, 2), E(4, 3))
     ag_finish(1, xs.at[1])
-    normalize(1, 1)
+    normalize(1, 1, nrm)
     arrived(3)
-    ext[1, 8:] = project(2).astype(F32)
+    ext[1, 8:] = project(2, nrm).astype(F32)
     send_halo(1)
-    mid_do(M(4, 1), M(4, 0))
+    mid_do(M(5, 0), M(5, 2), lambda: own_out_if(5, True))
+    end_do(E(5, 1))
     take_halo(1)
     gates(1, 0)
-    mid_do(M(4, 2), lambda: own_out_if(5, False))
-    end_do(E(4, 2))
     gates(1, 1)
     send_carry(1)
-    mid_do(M(5, 1), M(5, 0), M(5, 2), lambda: own_out_if(5, True))
-    end_do(E(4, 3))
+    end_do(E(5, 2))
     arrived(4)
-    gel_s[...] = jax.nn.gelu(project(3).astype(F32))
+    gel_s[...] = jax.nn.gelu(project(3, nrm).astype(F32))
     take_carry(1)
     mix()
 
     def ahead_last(i):
-        end_do(E(5, i))
+        if i == 1:
+            end_do(E(5, 3))
 
     project_out(1, ahead_last)
     close_layer(1, xs.at[1])
@@ -759,18 +823,26 @@
     inv = jnp.broadcast_to(inv, (128, rows)).T[:, 0:1]
     out_ref[...] = (xs[layers].astype(F32) * inv * final_ref[...]).astype(BF16)
 
+    assert not end_line and not mid_in_line
     close_weights()
-    at_end(lambda: lend_rows().wait_send())
+
+    @at_end
+    def _():
+        for h in range(BANDS):
+            lend_rows(h).wait_send()
 
     @at_mid
     def _():
+        ag_close(0, x_ref)
         ag_close(layers, agx.at[layers, t])
-        lend_back().wait_send()
+        for i in range(len(LENT)):
+            lend_back(i).wait_send()
 
     for layer in range(layers):
-        ag_close(layer, x_ref if layer == 0 else xs.at[layer])
-
-        @pl.when(s < n_sp - 1)
+        if layer:
+            ag_close(layer, xs.at[layer])
+
+        @pl.when((s >= first_sender(layer)) & (s < n_sp - 1))
         def _():
             halo_copy(layer).wait_send()
 
@@ -780,10 +852,11 @@
             def _():
                 carry_copy(layer, d).wait_send()
 
-        for q in range(chips):
-            near_copy(layer, q).wait_send()
-        for q in range(1, chips):
-            far_copy(layer, q).wait_send()
+        for h in range(BANDS):
+            for q in range(chips):
+                near_copy(layer, q, h).wait_send()
+            for q in range(1, chips):
+                far_copy(layer, q, h).wait_send()
     for d in range(1, n_tp):
         sq_copy(d).wait_send()
 
@@ -827,14 +900,15 @@
             pltpu.VMEM((layers + 1, n_tp, rows, feats), BF16),
             pltpu.VMEM((layers + 1, rows, feats), BF16),
             pltpu.VMEM((rows, n_tp * feats), BF16),
+            pltpu.VMEM((rows, n_tp * feats), BF16),
             pltpu.VMEM((layers, 8 + rows, chans), F32),
             pltpu.VMEM((layers, 8, chans), F32),
             pltpu.VMEM((rows, chans), F32),
             pltpu.VMEM((rows, chans), F32),
             pltpu.VMEM((rows, chans), F32),
             pltpu.VMEM((rows, chans), BF16),
-            pltpu.VMEM((rows, chans), BF16),
-            pltpu.VMEM((rows, chans), BF16),
+            pltpu.VMEM((len(LENT), rows, chans), BF16),
+            pltpu.VMEM((len(LENT), rows, chans), BF16),
             pltpu.VMEM((layers, n_tp, rows, feats), BF16),
             pltpu.VMEM((layers, chips, rows, feats), BF16),
             pltpu.VMEM((layers, chips, rows, feats), BF16),
@@ -848,11 +922,11 @@
             dma((count,)),
             dma((count, n_sp, 2, PARTS)),
             dma((3,)),
-            dma((3,)),
-            dma((layers + 1, 2 * chips)),
-            dma((layers + 1, n_tp)),
-            dma((layers, 2 * chips)),
-            dma((layers, 2 * chips)),
+            dma((BANDS + 2 * len(LENT),)),
+            dma((layers + 1, 2 * chips, BANDS)),
+            dma((layers + 1, n_tp, BANDS)),
+            dma((layers, 2 * chips, BANDS)),
+            dma((layers, 2 * chips, BANDS)),
             dma((layers, 2)),
             dma((layers, n_sp)),
             dma((layers, n_sp)),

time: 171 us -> 130 us (0.76)
  Pallas kernels: 167 us -> 126 us
    pallas_call x1, Pallas kernels: 167 us -> 126 us  [in_one_kernel(): pl.pallas_call(functools.partial(fused, sizes), out_shape=jax.ShapeDtypeS...]
where the time goes in v2:
time: 130 us
  Pallas kernels  126 us (97%)
  local copies, waits for them, and re-layouts  3.04 us (2%)
    pallas_call x1, Pallas kernels, in_one_kernel(): pl.pallas_call(functools.partial(fused, sizes), out_shape=jax.ShapeDtypeS...  126 us

profile of v2, /device:TPU:0, one launch (start us, length us, event | category | flops | bytes accessed | tf_op | source)
XLA Modules:
  0.0 130.0 jit_solution(1375625007315705682)
XLA Ops:
  0.0 0.0 copy-start.1
  0.0 0.0 copy-start
  0.0 0.7 copy-done.1
  0.7 0.6 reshape.18.mult_ref
  1.3 0.0 copy-done
  1.3 0.6 fusion.rate_ref
  1.9 126.3 %shard_map.118 = bf16[384,512]{1,0:T(8,128)(2,1)} custom-call(bf16[384,512]{1,0:T(8,128)(2,1)} %x_ref.1, bf16[2,2,256,512]{3,2,1,0:T(8,128)(2,1)} %bitcast.4, bf16[2,2,256,512]{3,2,1,0:T(8,128)(2,1)} %bitcast.5, bf16[2,2,256,512]{3,2,1,0:T(8,128)(2,1)} %bitcast.6, bf16[2,4,512]{2,1,0:T(4,128)(2,1)} %taps_ref.1, bf16[2,2,256,256]{3,2,1,0:T(8,128)(2,1)} %reset_w.1, ...), custom_call_target="tpu_custom_call" | custom-call | tf_op jit(solution)/shard_map/pallas_call | solution.py:892
  128.2 1.8 %copy.14 = bf16[384,512]{1,0:T(8,128)(2,1)} copy(bf16[384,512]{1,0:T(8,128)(2,1)} %shard_map.118) | data formatting | bytes 786432
Async XLA Ops:
  0.0 0.7 copy-start.1
  0.0 1.3 copy-start

commit v3 on v2

--- a/solution.py
+++ b/solution.py
@@ -156,6 +156,14 @@
     return jnp.where(u > -0.35, series, 1.0 - jnp.exp(u))
 
 
+def soft_plus(u):
+    e = jnp.exp(-jnp.abs(u))
+    series = jnp.zeros_like(e)
+    for k in range(10, 0, -1):
+        series = e * (1.0 / k - series)
+    return jnp.maximum(u, 0.0) + jnp.where(e < 0.1, series, jnp.log(1.0 + e))
+
+
 def shifted(value, steps, fill):
     rows = value.shape[0]
     if steps % 8 == 0:
@@ -167,10 +175,20 @@
 
 def fused(
     sizes,
-    x_ref,
+    x_hbm,
     branch_w,
     memory_w,
     exit_w,
+    taps_hbm,
+    reset_hbm,
+    inject_hbm,
+    forget_hbm,
+    mult_hbm,
+    spike_hbm,
+    gains_hbm,
+    final_hbm,
+    out_ref,
+    x_ref,
     taps_ref,
     reset_w,
     inject_w,
@@ -179,7 +197,6 @@
     spike_ref,
     gains_ref,
     final_ref,
-    out_ref,
     win,
     wout,
     agx,
@@ -204,8 +221,10 @@
     mult_s,
     sq_out,
     sq_in,
+    sem_load,
     sem_own,
-    sem_w_recv,
+    sem_piece,
+    sem_rest,
     sem_w_send,
     sem_lend,
     sem_ag_send,
@@ -236,6 +255,33 @@
     def at_mid(body):
         pl.when(is_mid)(body)
 
+    def own_block(m):
+        return (memory_w, branch_w, exit_w)[m % 3].at[m // 3]
+
+    def slot(m, j):
+        kind = 2 * (m // 3) + m % 3 if m % 3 < 2 else m // 3
+        return (win if m % 3 < 2 else wout), (kind * n_sp + j) * 2
+
+    def keep_own(m):
+        ref, at = slot(m, s)
+        return pltpu.make_async_copy(own_block(m), ref.at[pl.ds(at, 2)], sem_own.at[m])
+
+    loads = [
+        pltpu.make_async_copy(src, dst, sem_load.at[i])
+        for i, (src, dst) in enumerate(
+            (
+                (x_hbm, x_ref),
+                (gains_hbm, gains_ref),
+                (mult_hbm, mult_ref),
+                (forget_hbm, rate_ref),
+                (taps_hbm, taps_ref),
+                (reset_hbm, reset_w),
+                (inject_hbm, inject_w),
+                (spike_hbm, spike_ref),
+                (final_hbm, final_ref),
+            )
+        )
+    ]
     barrier = pltpu.get_barrier_semaphore()
     for d in range(1, n_tp):
         pl.semaphore_signal(
@@ -246,6 +292,10 @@
             barrier, inc=1, device_id={"sp": lax.rem(s + d, n_sp)}, device_id_type=MESH
         )
     pl.semaphore_signal(barrier, inc=1, device_id={"grp": 1 - g}, device_id_type=MESH)
+    for load in loads:
+        load.start()
+    for m in range(len(LENT), 3 * layers):
+        keep_own(m).start()
     pl.semaphore_wait(barrier, n_tp - 1 + n_sp - 1 + 1)
 
     IN, OUT, ACROSS = 0, 1, 2
@@ -255,13 +305,6 @@
             return {"grp": 1 - g}
         return {"sp": s + inw} if way == IN else {"sp": s - inw}
 
-    def own_block(m):
-        return (memory_w, branch_w, exit_w)[m % 3].at[m // 3]
-
-    def slot(m, j):
-        kind = 2 * (m // 3) + m % 3 if m % 3 < 2 else m // 3
-        return (win if m % 3 < 2 else wout), (kind * n_sp + j) * 2
-
     def cut(ref, q):
         size = ref.shape[0] // PARTS
         return ref.at[pl.ds(q * size, size)]
@@ -270,12 +313,17 @@
         ref, at = slot(m, j)
         return cut(ref.at[at + half], q)
 
-    def sent(src, m, j, half, q, way):
+    def arrival(m, j, place, mine, q):
+        away = lax.rem(j - place + 2 * n_sp - 1, n_sp)
+        return sem_piece.at[m, away, q] if mine else sem_rest.at[m, away]
+
+    def sent(src, m, j, half, q, way, mine):
+        place = s + (inw, -inw, 0)[way]
         return pltpu.make_async_remote_copy(
             src_ref=src,
             dst_ref=held(m, j, half, q),
             send_sem=sem_w_send.at[way],
-            recv_sem=sem_w_recv.at[m, j, half, q],
+            recv_sem=arrival(m, j, place, mine, q),
             device_id=target(way),
             device_id_type=MESH,
         )
@@ -283,13 +331,15 @@
     def relay(m, j, q, ways):
         src = held(m, j, g, q)
         for way in ways:
-            sent(src, m, j, g, q, way).start()
-
-    def landed(m, j, half, q):
-        sent(held(m, j, half, q), m, j, half, q, ACROSS).wait_recv()
+            sent(src, m, j, g, q, way, way != ACROSS).start()
+
+    def landed(m, j, q):
+        piece = held(m, j, g, q)
+        sent(piece, m, j, g, q, ACROSS, True).wait_recv()
 
     def own(m, way, half, q):
-        sent(cut(own_block(m).at[half], q), m, s, half, q, way).start()
+        src = cut(own_block(m).at[half], q)
+        sent(src, m, s, half, q, way, half is g).start()
 
     def own_both(m, way):
         for q in range(PARTS):
@@ -300,7 +350,7 @@
         halves += [(m, g), (m - 1, 1 - g)]
     halves.append((count - 1, 1 - g))
     end_line = [(m, half, q) for m, half in halves for q in range(PARTS)]
-    mid_in_line = [(m, q) for m in range(1, count) for q in range(PARTS)]
+    mid_in_line = [(m, q) for m in (2, 1, *range(3, count)) for q in range(PARTS)]
     def feed_end(steps):
         steps *= PARTS // 2
         for m, half, q in end_line[:steps]:
@@ -312,38 +362,26 @@
             own(m, IN, g, q)
         del mid_in_line[:steps]
 
-    def keep_own(m):
-        ref, at = slot(m, s)
-        return pltpu.make_async_copy(own_block(m), ref.at[pl.ds(at, 2)], sem_own.at[m])
-
-    def late():
-        return chip == (s + is_end.astype(jnp.int32) * inw) // (n_tp // chips)
-
-    def end_turn(i):
-        return lax.rem(i - 1 + late().astype(jnp.int32), n_sp - 1) + 1
-
-    def own_out_if(m, when):
-        @pl.when(late() if when else jnp.logical_not(late()))
-        def _():
-            own_both(m, OUT)
-
-    def end_pump(m, i, feed):
-        j = s + inw * (end_turn(i) if m == count - 1 else i)
-        for q in range(PARTS):
-            landed(m, j, g, q)
+    def end_pump(m, i, feed, pieces=range(PARTS)):
+        j = s + inw * i
+        for q in pieces:
+            landed(m, j, q)
             relay(m, j, q, (ACROSS,))
             if q % (PARTS // 2) == PARTS // 2 - 1:
                 feed_end(feed)
 
-    def mid_pump(m, k, feed):
-        j = s + inw * (k if k else -1)
-        for q in range(PARTS):
-            landed(m, j, g, q)
-            if k == 0:
-                ways = (IN,) if m in WHOLE else (IN, ACROSS)
-            else:
-                ways = (ACROSS,) if m in LENT else (OUT, ACROSS)
-            relay(m, j, q, ways)
+    def mid_block(k):
+        return s + inw * (k if k else -1)
+
+    def mid_ways(m, k):
+        if k == 0:
+            return (IN,) if m in WHOLE else (IN, ACROSS)
+        return (ACROSS,) if m in LENT else (OUT, ACROSS)
+
+    def mid_pump(m, k, feed, pieces=range(PARTS)):
+        for q in pieces:
+            landed(m, mid_block(k), q)
+            relay(m, mid_block(k), q, mid_ways(m, k))
         feed_in(feed)
 
     def end_do(*acts):
@@ -370,8 +408,16 @@
         return lambda: feed_end(steps)
 
     def ready(m, j):
-        for q in range(PARTS):
-            landed(m, j, 1 - g, q)
+        ref, at = slot(m, j)
+        rest = ref.at[at + 1 - g]
+        pltpu.make_async_remote_copy(
+            src_ref=rest,
+            dst_ref=rest,
+            send_sem=sem_w_send.at[ACROSS],
+            recv_sem=arrival(m, j, s, False, 0),
+            device_id=target(ACROSS),
+            device_id_type=MESH,
+        ).wait_recv()
 
     def arrived(m):
         keep_own(m).wait()
@@ -384,7 +430,7 @@
             src_ref=view,
             dst_ref=view,
             send_sem=sem_w_send.at[way],
-            recv_sem=sem_w_recv.at[0, 0, 0, 0],
+            recv_sem=sem_rest.at[0, 0],
             device_id=target(ACROSS),
             device_id_type=MESH,
         ).wait_send()
@@ -406,11 +452,11 @@
     def band(ref, h):
         return ref.at[pl.ds(h * (rows // BANDS), rows // BANDS)]
 
-    def ag_copy(src, layer, owner, k, h, where):
+    def ag_copy(src, layer, owner, h, where):
         return pltpu.make_async_remote_copy(
             src_ref=band(src, h),
             dst_ref=band(agx.at[layer, owner], h),
-            send_sem=sem_ag_send.at[layer, k, h],
+            send_sem=sem_ag_send.at[layer],
             recv_sem=sem_ag_recv.at[layer, owner, h],
             device_id={"tp": where},
             device_id_type=MESH,
@@ -418,28 +464,36 @@
 
     def ag_start(layer, src, h):
         for d in range(1, chips):
-            ag_copy(src, layer, t, d, h, lax.rem(t + 2 * d, n_tp)).start()
-        ag_copy(src, layer, t, 0, h, sib).start()
-
-    def ag_finish(layer, src):
+            ag_copy(src, layer, t, h, lax.rem(t + 2 * d, n_tp)).start()
+        ag_copy(src, layer, t, h, sib).start()
+
+    def ag_forward(layer):
         for h in range(BANDS):
             for d in range(1, chips):
                 owner = lax.rem(t + 2 * d, n_tp)
                 block = agx.at[layer, owner]
-                ag_copy(block, layer, owner, d, h, sib).wait_recv()
-                ag_copy(block, layer, owner, chips + d, h, sib).start()
+                ag_copy(block, layer, owner, h, sib).wait_recv()
+                ag_copy(block, layer, owner, h, sib).start()
+
+    def ag_finish(layer, src):
         for h in range(BANDS):
-            ag_copy(src, layer, sib, 0, h, sib).wait_recv()
+            ag_copy(src, layer, sib, h, sib).wait_recv()
             for d in range(1, chips):
                 owner = lax.rem(sib + 2 * d, n_tp)
-                ag_copy(agx.at[layer, owner], layer, owner, d, h, sib).wait_recv()
-
-    def ag_close(layer, src):
-        for h in range(BANDS):
-            for d in range(1, chips):
-                ag_copy(src, layer, t, d, h, sib).wait_send()
-                ag_copy(src, layer, t, chips + d, h, sib).wait_send()
-            ag_copy(src, layer, t, 0, h, sib).wait_send()
+                ag_copy(agx.at[layer, owner], layer, owner, h, sib).wait_recv()
+
+    def wait_blocks(view, sem):
+        pltpu.make_async_remote_copy(
+            src_ref=view,
+            dst_ref=view,
+            send_sem=sem,
+            recv_sem=sem_rest.at[0, 0],
+            device_id=target(ACROSS),
+            device_id_type=MESH,
+        ).wait_send()
+
+    def ag_close(layer):
+        wait_blocks(agx.at[layer, pl.ds(0, 2 * chips - 1)], sem_ag_send.at[layer])
 
     def lend_rows(h):
         return pltpu.make_async_remote_copy(
@@ -526,7 +580,7 @@
         return pltpu.make_async_remote_copy(
             src_ref=src,
             dst_ref=dst,
-            send_sem=sem_rs_send.at[layer, k, h],
+            send_sem=sem_rs_send.at[layer],
             recv_sem=sem_rs_recv.at[layer, k, h],
             device_id={"tp": where},
             device_id_type=MESH,
@@ -540,7 +594,7 @@
     def far_copy(layer, q, h):
         where = lax.rem(t + 2 * q, n_tp)
         src, dst = band(pair.at[layer, q], h), band(from_far.at[layer, q], h)
-        return rs_copy(src, dst, layer, chips + q, h, where)
+        return rs_copy(src, dst, layer, chips + q - 1, h, where)
 
     def first_sender(layer):
         return 1 if layer == 0 else 0
@@ -647,28 +701,38 @@
                 ).astype(BF16)
                 far_copy(layer, q, h).start()
 
-    def exit_order(layer, i):
-        end_step = end_turn(i) if layer == layers - 1 else i
-        mid_step = (-1, 1, 2)[i - 1]
-        e = is_end.astype(jnp.int32)
-        return s + inw * (e * end_step + (1 - e) * mid_step)
+    def crossing_order(i):
+        there = 2 * (1 - chip) if i < 2 else 2 * chip
+        return there + (core if i % 2 else 1 - core)
 
     def project_out(layer, ahead):
         m = 3 * layer + 2
+        e = is_end.astype(jnp.int32)
+        turned = (chip == s // (n_tp // chips)).astype(jnp.int32)
         keep_own(m).wait()
-        product(layer, s)
-        before = s
-        for i in range(1, n_sp):
+
+        @at_mid
+        def _():
+            for d in range(1, n_sp):
+                ready(m, lax.rem(s + d, n_sp))
+
+        waiting = []
+        for i in range(n_sp):
+            step = (0, 1, 2, 3)[i] + turned * (2, -1, -1, 0)[i]
+            j = s + inw * step
             ahead(i)
-            j = exit_order(layer, i)
-            ready(m, j)
+            pl.when(is_end & (step > 0))(functools.partial(ready, m, j))
+            j = crossing_order(i) + e * (j - crossing_order(i))
             product(layer, j)
-            pass_on(layer, before)
-            before = j
-        pass_on(layer, before)
-
-    def close_layer(layer, src):
+            waiting.append(j)
+            if i:
+                for done in waiting:
+                    pass_on(layer, done)
+                waiting = []
+
+    def close_layer(layer, src, ahead):
         for h in range(BANDS):
+            ahead(h)
             at = pl.ds(h * (rows // BANDS), rows // BANDS)
             near_copy(layer, 0, h).wait_recv()
             mixed = part[layer, t, at].astype(F32) + from_sib[layer, 0, at].astype(F32)
@@ -680,6 +744,7 @@
                 ag_start(layer + 1, xs.at[layer + 1], h)
 
     own_both(0, IN)
+    loads[0].wait()
 
     @at_end
     def _():
@@ -691,20 +756,22 @@
     def _():
         for h in range(BANDS):
             ag_start(0, x_ref, h)
-        for m in (2, 3, 4):
+        for m in range(len(LENT), count - 1):
             own_both(m, OUT)
         for m in LENT:
             keep_own(m).start()
         agx[0, t] = x_ref[...]
 
-    for m in range(len(LENT), count):
-        keep_own(m).start()
-    mult_s[...] = jnp.broadcast_to(mult_ref[...], (128, rows)).T[:, 0:1]
+    for load in loads[1:]:
+        load.wait()
+    rate_ref[...] = -SQUASH_POWER * soft_plus(-rate_ref[...])
+    mult_s[...] = jnp.broadcast_to(mult_ref[...].reshape(1, rows), (128, rows)).T[:, 0:1]
 
     @at_mid
     def _():
         mid_pump(0, 0, PARTS)
         mid_pump(0, 1, 0)
+        ag_forward(0)
         ag_finish(0, x_ref)
         normalize(0, 0, nrm)
         lend_rows(0).wait_recv()
@@ -713,18 +780,27 @@
         for h in range(1, BANDS):
             lend_rows(h).wait_recv()
             ag_start(layers, agx.at[layers, t], h)
-        mid_pump(1, 1, 0)
-        mid_pump(1, 0, 0)
+        for q in range(PARTS):
+            landed(2, mid_block(1), q)
+            relay(2, mid_block(1), q, (OUT,))
+        own_both(count - 1, OUT)
+        ag_forward(layers)
         arrived(0)
         ext[0, 8:] = project(0, nrm).astype(F32)
         send_halo(0)
-        mid_pump(2, 1, 0)
+        for q in range(PARTS):
+            landed(1, mid_block(1), q)
+            relay(1, mid_block(1), q, mid_ways(1, 1))
+            landed(1, mid_block(0), q)
+            relay(1, mid_block(0), q, mid_ways(1, 0))
         ag_finish(layers, agx.at[layers, t])
         normalize(layers, 0, nrm_lent)
         lent_out[0] = project(0, nrm_lent)
         lend_back(0).start()
         mid_pump(2, 0, PARTS)
         mid_pump(1, 2, 0)
+        for q in range(PARTS):
+            relay(2, mid_block(1), q, (ACROSS,))
 
     @at_end
     def _():
@@ -734,6 +810,7 @@
         feed_end(2)
         end_pump(2, 2, 1)
         feed_end(2)
+        end_pump(5, 1, 0)
         lend_back(0).wait_recv()
         ext[0, 8:] = lent_in[0].astype(F32)
 
@@ -744,10 +821,11 @@
 
     @at_mid
     def _():
-        mid_pump(2, 2, 0)
+        mid_pump(2, 2, 0, range(PARTS // 2))
         arrived(1)
         lent_out[1] = project(1, nrm_lent)
         lend_back(1).start()
+        mid_pump(2, 2, 0, range(PARTS // 2, PARTS))
         gel_s[...] = jax.nn.gelu(project(1, nrm).astype(F32))
         mid_pump(3, 1, 0)
         mid_pump(3, 0, PARTS)
@@ -755,7 +833,7 @@
     @at_end
     def _():
         feed_end(4)
-        end_pump(2, 3, 0)
+        end_pump(2, 3, 0, range(PARTS // 2))
         lend_back(1).wait_recv()
         feed_end(2)
         gel_s[...] = jax.nn.gelu(lent_in[1].astype(F32))
@@ -763,41 +841,76 @@
     take_carry(0)
     mix()
 
-    def ahead(i):
-        if i == 3:
-            mid_do(M(3, 2), M(4, 1))
-
-    project_out(0, ahead)
-    mid_do(M(4, 0, PARTS))
-    end_do(F(2))
-    close_layer(0, x_ref)
+    last_pieces = [
+        (m, i, q) for m, i in ((4, 3), (5, 2), (5, 3)) for q in range(PARTS)
+    ]
+
+    def end_last(steps):
+        @at_end
+        def _():
+            for m, i, q in last_pieces[:steps]:
+                landed(m, s + inw * i, q)
+                relay(m, s + inw * i, q, (ACROSS,))
+
+        del last_pieces[:steps]
+
+    def nothing(_):
+        return
+
+    def between(h):
+        if h == 0:
+            end_do(F(2), lambda: end_pump(3, 2, 0, range(PARTS // 2, PARTS)))
+            mid_do(M(3, 2))
+        turned = chip == s // (n_tp // chips)
+        if h == 0:
+            pl.when(is_end & jnp.logical_not(turned))(E(3, 3))
+        if h == BANDS - 1:
+            pl.when(is_end & turned)(E(3, 3))
+            mid_do(M(4, 1), M(4, 0, PARTS))
+
+    def rest_ahead(i):
+        if i == n_sp - 1:
+            end_do(lambda: end_pump(2, 3, 0, range(PARTS // 2, PARTS)), F(2))
+            end_do(lambda: end_pump(3, 2, 0, range(PARTS // 2)))
+
+    project_out(0, rest_ahead)
+    close_layer(0, x_ref, between)
 
     agx[1, t] = xs[1]
-    mid_do(M(4, 2), lambda: own_out_if(5, False), M(5, 1))
-    end_do(E(3, 2, 1), E(3, 3), F(99), E(4, 2), E(4, 3))
+    mid_do(M(4, 2), M(5, 0))
+    end_do(F(99), E(4, 2))
+    end_last(1)
+    ag_forward(1)
     ag_finish(1, xs.at[1])
+    end_last(1)
     normalize(1, 1, nrm)
+    end_last(1)
     arrived(3)
     ext[1, 8:] = project(2, nrm).astype(F32)
     send_halo(1)
-    mid_do(M(5, 0), M(5, 2), lambda: own_out_if(5, True))
-    end_do(E(5, 1))
+    mid_do(M(5, 1))
+    pl.when(s == 1)(M(5, 2))
+    end_last(1)
     take_halo(1)
     gates(1, 0)
+    end_last(1)
     gates(1, 1)
     send_carry(1)
-    end_do(E(5, 2))
+    pl.when(is_mid & (s > 1))(M(5, 2))
+    end_last(1)
     arrived(4)
+    end_last(1)
     gel_s[...] = jax.nn.gelu(project(3, nrm).astype(F32))
+    end_last(2)
     take_carry(1)
     mix()
 
-    def ahead_last(i):
-        if i == 1:
-            end_do(E(5, 3))
-
-    project_out(1, ahead_last)
-    close_layer(1, xs.at[1])
+    def last_ahead(i):
+        if i < n_sp - 1:
+            end_last(1)
+
+    project_out(1, last_ahead)
+    close_layer(1, xs.at[1], nothing)
 
     fresh = xs[layers].astype(F32)
     square = jnp.sum(fresh * fresh, axis=1, keepdims=True)
@@ -823,7 +936,7 @@
     inv = jnp.broadcast_to(inv, (128, rows)).T[:, 0:1]
     out_ref[...] = (xs[layers].astype(F32) * inv * final_ref[...]).astype(BF16)
 
-    assert not end_line and not mid_in_line
+    assert not end_line and not mid_in_line and not last_pieces
     close_weights()
 
     @at_end
@@ -833,14 +946,14 @@
 
     @at_mid
     def _():
-        ag_close(0, x_ref)
-        ag_close(layers, agx.at[layers, t])
+        ag_close(0)
+        ag_close(layers)
         for i in range(len(LENT)):
             lend_back(i).wait_send()
 
     for layer in range(layers):
         if layer:
-            ag_close(layer, xs.at[layer])
+            ag_close(layer)
 
         @pl.when((s >= first_sender(layer)) & (s < n_sp - 1))
         def _():
@@ -852,11 +965,7 @@
             def _():
                 carry_copy(layer, d).wait_send()
 
-        for h in range(BANDS):
-            for q in range(chips):
-                near_copy(layer, q, h).wait_send()
-            for q in range(1, chips):
-                far_copy(layer, q, h).wait_send()
+        wait_blocks(part.at[layer, pl.ds(0, 2 * chips - 1)], sem_rs_send.at[layer])
     for d in range(1, n_tp):
         sq_copy(d).wait_send()
 
@@ -884,7 +993,6 @@
     chips = n_tp // 2
     half_in = (layers, 2, depth // 2, chans)
     half_out = (layers, 2, chans // 2, depth)
-    rate = -SQUASH_POWER * jax.nn.softplus(-forgetting_parameters)
     vmem = pl.BlockSpec(memory_space=pltpu.VMEM)
     hbm = pl.BlockSpec(memory_space=pl.ANY)
     count = 3 * layers
@@ -892,9 +1000,18 @@
     return pl.pallas_call(
         functools.partial(fused, sizes),
         out_shape=jax.ShapeDtypeStruct((rows, feats), BF16),
-        in_specs=[vmem, hbm, hbm, hbm] + [vmem] * 8,
+        in_specs=[hbm] * 12,
         out_specs=vmem,
         scratch_shapes=[
+            pltpu.VMEM((rows, feats), BF16),
+            pltpu.VMEM(filter_coefficients.shape, BF16),
+            pltpu.VMEM(memory_valve_matrix.shape, BF16),
+            pltpu.VMEM(entry_valve_matrix.shape, BF16),
+            pltpu.VMEM((layers, chans), F32),
+            pltpu.VMEM((rows,), F32),
+            pltpu.VMEM((rows, chans), F32),
+            pltpu.VMEM((layers, n_tp * feats), F32),
+            pltpu.VMEM((1, feats), F32),
             pltpu.VMEM((2 * layers * n_sp * 2, depth // 2, chans), BF16),
             pltpu.VMEM((layers * n_sp * 2, chans // 2, depth), BF16),
             pltpu.VMEM((layers + 1, n_tp, rows, feats), BF16),
@@ -919,14 +1036,16 @@
             pltpu.VMEM((rows, 1), F32),
             pltpu.VMEM((8, rows), F32),
             pltpu.VMEM((n_tp, 8, rows), F32),
+            dma((9,)),
             dma((count,)),
-            dma((count, n_sp, 2, PARTS)),
+            dma((count, n_sp - 1, PARTS)),
+            dma((count, n_sp - 1)),
             dma((3,)),
             dma((BANDS + 2 * len(LENT),)),
-            dma((layers + 1, 2 * chips, BANDS)),
+            dma((layers + 1,)),
             dma((layers + 1, n_tp, BANDS)),
-            dma((layers, 2 * chips, BANDS)),
-            dma((layers, 2 * chips, BANDS)),
+            dma((layers,)),
+            dma((layers, 2 * chips - 1, BANDS)),
             dma((layers, 2)),
             dma((layers, n_sp)),
             dma((layers, n_sp)),
@@ -944,8 +1063,8 @@
         filter_coefficients,
         memory_valve_matrix,
         entry_valve_matrix,
-        rate,
-        timestep_forgetting_multiplier.reshape(1, rows),
+        forgetting_parameters,
+        timestep_forgetting_multiplier,
         spike_extra,
         prelude_rms_gains,
         finishing_rms_gains.reshape(1, feats),

time: 130 us -> 113 us (0.87)
  Pallas kernels: 126 us -> 111 us
    pallas_call x1, Pallas kernels: 126 us -> 111 us  [in_one_kernel(): pl.pallas_call(functools.partial(fused, sizes), out_shape=jax.ShapeDtypeS...]
where the time goes in v3:
time: 113 us
  Pallas kernels  111 us (98%)
  local copies, waits for them, and re-layouts  1.77 us (2%)
    pallas_call x1, Pallas kernels, in_one_kernel(): pl.pallas_call(functools.partial(fused, sizes), out_shape=jax.ShapeDtypeS...  111 us

profile of v3, /device:TPU:0, one launch (start us, length us, event | category | flops | bytes accessed | tf_op | source)
XLA Modules:
  0.0 112.7 jit_solution(2886754654924049268)
XLA Ops:
  0.0 111.0 %shard_map.118 = bf16[384,512]{1,0:T(8,128)(2,1)} custom-call(bf16[384,512]{1,0:T(8,128)(2,1)} %x_hbm.1, bf16[2,2,256,512]{3,2,1,0:T(8,128)(2,1)} %bitcast.4, bf16[2,2,256,512]{3,2,1,0:T(8,128)(2,1)} %bitcast.5, bf16[2,2,256,512]{3,2,1,0:T(8,128)(2,1)} %bitcast.6, bf16[2,4,512]{2,1,0:T(4,128)(2,1)} %taps_hbm.1, bf16[2,2,256,256]{3,2,1,0:T(8,128)(2,1)} %reset_hbm.1, ...), custom_call_target="tpu_custom_call" | custom-call | tf_op jit(solution)/shard_map/pallas_call | solution.py:1000
  111.0 1.8 %copy.14 = bf16[384,512]{1,0:T(8,128)(2,1)} copy(bf16[384,512]{1,0:T(8,128)(2,1)} %shard_map.118) | data formatting | bytes 786432

commit v4 on v3

--- a/solution.py
+++ b/solution.py
@@ -255,22 +255,38 @@
     def at_mid(body):
         pl.when(is_mid)(body)
 
-    def own_block(m):
-        return (memory_w, branch_w, exit_w)[m % 3].at[m // 3]
+    width = feats // 2
+
+    def own_half(m, half):
+        if m % 3 < 2:
+            return (memory_w, branch_w)[m % 3].at[m // 3, half]
+        cols = pl.ds(pl.multiple_of(half * width, width), width)
+        return exit_w.at[m // 3, :, cols]
 
     def slot(m, j):
         kind = 2 * (m // 3) + m % 3 if m % 3 < 2 else m // 3
         return (win if m % 3 < 2 else wout), (kind * n_sp + j) * 2
 
+    def keep_half(m, half):
+        ref, at = slot(m, s)
+        return pltpu.make_async_copy(
+            own_half(m, half), ref.at[at + half], sem_own.at[m, half]
+        )
+
     def keep_own(m):
-        ref, at = slot(m, s)
-        return pltpu.make_async_copy(own_block(m), ref.at[pl.ds(at, 2)], sem_own.at[m])
+        for half in range(2):
+            keep_half(m, half).start()
+
+    def kept(m):
+        for half in range(2):
+            keep_half(m, half).wait()
 
     loads = [
         pltpu.make_async_copy(src, dst, sem_load.at[i])
         for i, (src, dst) in enumerate(
             (
-                (x_hbm, x_ref),
+                (x_hbm.at[:, 0:width], x_ref.at[0]),
+                (x_hbm.at[:, width:], x_ref.at[1]),
                 (gains_hbm, gains_ref),
                 (mult_hbm, mult_ref),
                 (forget_hbm, rate_ref),
@@ -295,7 +311,7 @@
     for load in loads:
         load.start()
     for m in range(len(LENT), 3 * layers):
-        keep_own(m).start()
+        keep_own(m)
     pl.semaphore_wait(barrier, n_tp - 1 + n_sp - 1 + 1)
 
     IN, OUT, ACROSS = 0, 1, 2
@@ -338,7 +354,7 @@
         sent(piece, m, j, g, q, ACROSS, True).wait_recv()
 
     def own(m, way, half, q):
-        src = cut(own_block(m).at[half], q)
+        src = cut(own_half(m, half), q)
         sent(src, m, s, half, q, way, half is g).start()
 
     def own_both(m, way):
@@ -420,7 +436,7 @@
         ).wait_recv()
 
     def arrived(m):
-        keep_own(m).wait()
+        kept(m)
         for d in range(1, n_sp):
             ready(m, lax.rem(s + d, n_sp))
 
@@ -449,8 +465,11 @@
             wait_sends(OUT, (count - lent) * (n_sp - 1))
             wait_sends(ACROSS, count * (n_sp - 1) - whole)
 
+    def nth(h):
+        return 1 - g if h else g
+
     def band(ref, h):
-        return ref.at[pl.ds(h * (rows // BANDS), rows // BANDS)]
+        return ref.at[nth(h)]
 
     def ag_copy(src, layer, owner, h, where):
         return pltpu.make_async_remote_copy(
@@ -522,14 +541,16 @@
             at = pl.ds(pl.multiple_of(i * step, step), step)
             total = jnp.zeros((step, 1), F32)
             for p in range(n_tp):
-                f = agx[layer, p, at].astype(F32)
-                total = total + jnp.sum(f * f, axis=1, keepdims=True)
+                for c in range(2):
+                    f = agx[layer, p, c, at].astype(F32)
+                    total = total + jnp.sum(f * f, axis=1, keepdims=True)
             inv = lax.rsqrt(total / full + EPSILON)
             for p in range(n_tp):
-                cols = slice(p * feats, (p + 1) * feats)
-                f = agx[layer, p, at].astype(F32)
-                gain = gains_ref[gain_row : gain_row + 1, cols]
-                nrm[at, cols] = (f * inv * gain).astype(BF16)
+                for c in range(2):
+                    cols = slice(p * feats + c * width, p * feats + (c + 1) * width)
+                    f = agx[layer, p, c, at].astype(F32)
+                    gain = gains_ref[gain_row : gain_row + 1, cols]
+                    nrm[at, cols] = (f * inv * gain).astype(BF16)
             return carry
 
         lax.fori_loop(0, pieces, one, 0)
@@ -675,31 +696,29 @@
     def chips_on(j):
         return lax.rem(j // 2 - chip + chips, chips)
 
-    def product(layer, j):
-        at = (layer * n_sp + j) * 2
-        part[layer, j] = jnp.dot(
+    def product(layer, j, h):
+        half = nth(h)
+        part[layer, j, half] = jnp.dot(
             mix_s[...],
-            wout[pl.ds(at, 2)].reshape(chans, depth),
+            wout[(layer * n_sp + j) * 2 + half],
             preferred_element_type=F32,
         ).astype(BF16)
 
         @pl.when(lax.rem(j, 2) != core)
         def _():
-            for h in range(BANDS):
-                near_copy(layer, chips_on(j), h).start()
-
-    def pass_on(layer, j):
+            near_copy(layer, chips_on(j), h).start()
+
+    def pass_on(layer, j, h):
         q = chips_on(j)
+        half = nth(h)
 
         @pl.when((lax.rem(j, 2) == core) & (q != 0))
         def _():
-            for h in range(BANDS):
-                at = pl.ds(h * (rows // BANDS), rows // BANDS)
-                near_copy(layer, q, h).wait_recv()
-                pair[layer, q, at] = (
-                    part[layer, j, at].astype(F32) + from_sib[layer, q, at].astype(F32)
-                ).astype(BF16)
-                far_copy(layer, q, h).start()
+            near_copy(layer, q, h).wait_recv()
+            pair[layer, q, half] = (
+                part[layer, j, half].astype(F32) + from_sib[layer, q, half].astype(F32)
+            ).astype(BF16)
+            far_copy(layer, q, h).start()
 
     def crossing_order(i):
         there = 2 * (1 - chip) if i < 2 else 2 * chip
@@ -709,42 +728,58 @@
         m = 3 * layer + 2
         e = is_end.astype(jnp.int32)
         turned = (chip == s // (n_tp // chips)).astype(jnp.int32)
-        keep_own(m).wait()
+        kept(m)
 
         @at_mid
         def _():
             for d in range(1, n_sp):
                 ready(m, lax.rem(s + d, n_sp))
 
-        waiting = []
-        for i in range(n_sp):
+        def place(i):
             step = (0, 1, 2, 3)[i] + turned * (2, -1, -1, 0)[i]
-            j = s + inw * step
-            ahead(i)
-            pl.when(is_end & (step > 0))(functools.partial(ready, m, j))
-            j = crossing_order(i) + e * (j - crossing_order(i))
-            product(layer, j)
-            waiting.append(j)
-            if i:
-                for done in waiting:
-                    pass_on(layer, done)
-                waiting = []
+            arriving = s + inw * step
+            return step, arriving, crossing_order(i) + e * (arriving - crossing_order(i))
+
+        pair_of = []
+        for i in range(2):
+            step, arriving, j = place(i)
+            ahead(i, 0)
+            pl.when(is_end & (step > 0))(functools.partial(ready, m, arriving))
+            pair_of.append(j)
+        for h in range(BANDS):
+            for j in pair_of:
+                product(layer, j, h)
+            ahead(1, 1 + h)
+            for j in pair_of:
+                pass_on(layer, j, h)
+        for i in range(2, n_sp):
+            step, arriving, j = place(i)
+            ahead(i, 0)
+            product(layer, j, 0)
+            ahead(i, 1)
+            pass_on(layer, j, 0)
+            ahead(i, 2)
+            pl.when(is_end & (step > 0))(functools.partial(ready, m, arriving))
+            product(layer, j, 1)
+            ahead(i, 3)
+            pass_on(layer, j, 1)
 
     def close_layer(layer, src, ahead):
         for h in range(BANDS):
             ahead(h)
-            at = pl.ds(h * (rows // BANDS), rows // BANDS)
+            half = nth(h)
             near_copy(layer, 0, h).wait_recv()
-            mixed = part[layer, t, at].astype(F32) + from_sib[layer, 0, at].astype(F32)
+            mixed = part[layer, t, half].astype(F32) + from_sib[layer, 0, half].astype(F32)
             for q in range(1, chips):
                 far_copy(layer, q, h).wait_recv()
-                mixed = mixed + from_far[layer, q, at].astype(F32)
-            xs[layer + 1, at] = (src[at].astype(F32) + mixed).astype(BF16)
+                mixed = mixed + from_far[layer, q, half].astype(F32)
+            xs[layer + 1, half] = (src[half].astype(F32) + mixed).astype(BF16)
             if layer + 1 < layers:
                 ag_start(layer + 1, xs.at[layer + 1], h)
 
     own_both(0, IN)
-    loads[0].wait()
+    for load in loads[:2]:
+        load.wait()
 
     @at_end
     def _():
@@ -759,10 +794,10 @@
         for m in range(len(LENT), count - 1):
             own_both(m, OUT)
         for m in LENT:
-            keep_own(m).start()
+            keep_own(m)
         agx[0, t] = x_ref[...]
 
-    for load in loads[1:]:
+    for load in loads[2:]:
         load.wait()
     rate_ref[...] = -SQUASH_POWER * soft_plus(-rate_ref[...])
     mult_s[...] = jnp.broadcast_to(mult_ref[...].reshape(1, rows), (128, rows)).T[:, 0:1]
@@ -841,25 +876,29 @@
     take_carry(0)
     mix()
 
-    last_pieces = [
-        (m, i, q) for m, i in ((4, 3), (5, 2), (5, 3)) for q in range(PARTS)
-    ]
-
-    def end_last(steps):
-        @at_end
-        def _():
-            for m, i, q in last_pieces[:steps]:
-                landed(m, s + inw * i, q)
-                relay(m, s + inw * i, q, (ACROSS,))
-
-        del last_pieces[:steps]
+    def pieces_of(*runs):
+        return [(m, i, q) for m, i, first in runs for q in range(first, PARTS)]
+
+    early = [pieces_of((2, 3, PARTS // 2), (3, 2, 0)) for _ in range(2)]
+    final = [pieces_of((4, 3, 0), (5, 2, 0), (5, 3, 0)) for _ in range(2)]
+
+    def end_next(lists, even, odd):
+        for parity, steps in ((0, even), (1, odd)):
+            now = lists[parity][:steps]
+            del lists[parity][:steps]
+
+            @pl.when(is_end & (core == parity))
+            def _():
+                for m, i, q in now:
+                    landed(m, s + inw * i, q)
+                    relay(m, s + inw * i, q, (ACROSS,))
 
     def nothing(_):
         return
 
     def between(h):
         if h == 0:
-            end_do(F(2), lambda: end_pump(3, 2, 0, range(PARTS // 2, PARTS)))
+            end_do(F(2))
             mid_do(M(3, 2))
         turned = chip == s // (n_tp // chips)
         if h == 0:
@@ -868,10 +907,19 @@
             pl.when(is_end & turned)(E(3, 3))
             mid_do(M(4, 1), M(4, 0, PARTS))
 
-    def rest_ahead(i):
-        if i == n_sp - 1:
-            end_do(lambda: end_pump(2, 3, 0, range(PARTS // 2, PARTS)), F(2))
-            end_do(lambda: end_pump(3, 2, 0, range(PARTS // 2)))
+    def rest_ahead(i, stage):
+        even, odd = {
+            (1, 0): (0, 1),
+            (1, 1): (0, 2),
+            (2, 0): (1, 1),
+            (3, 0): (1, 0),
+            (3, 1): (1, 1),
+            (3, 2): (2, 1),
+            (3, 3): (1, 0),
+        }.get((i, stage), (0, 0))
+        end_next(early, even, odd)
+        if (i, stage) == (3, 0):
+            end_do(F(2))
 
     project_out(0, rest_ahead)
     close_layer(0, x_ref, between)
@@ -879,41 +927,44 @@
     agx[1, t] = xs[1]
     mid_do(M(4, 2), M(5, 0))
     end_do(F(99), E(4, 2))
-    end_last(1)
+    end_next(final, 1, 1)
     ag_forward(1)
+    end_next(final, 0, 3)
     ag_finish(1, xs.at[1])
-    end_last(1)
+    end_next(final, 1, 0)
     normalize(1, 1, nrm)
-    end_last(1)
+    end_next(final, 0, 1)
     arrived(3)
     ext[1, 8:] = project(2, nrm).astype(F32)
     send_halo(1)
     mid_do(M(5, 1))
     pl.when(s == 1)(M(5, 2))
-    end_last(1)
+    end_next(final, 1, 1)
     take_halo(1)
     gates(1, 0)
-    end_last(1)
+    end_next(final, 1, 1)
     gates(1, 1)
     send_carry(1)
     pl.when(is_mid & (s > 1))(M(5, 2))
-    end_last(1)
+    end_next(final, 2, 1)
     arrived(4)
-    end_last(1)
+    end_next(final, 1, 0)
     gel_s[...] = jax.nn.gelu(project(3, nrm).astype(F32))
-    end_last(2)
+    end_next(final, 2, 2)
     take_carry(1)
     mix()
 
-    def last_ahead(i):
-        if i < n_sp - 1:
-            end_last(1)
+    def last_ahead(i, stage):
+        even, odd = {(0, 0): (1, 2), (1, 1): (1, 0), (2, 0): (1, 0)}.get((i, stage), (0, 0))
+        end_next(final, even, odd)
 
     project_out(1, last_ahead)
     close_layer(1, xs.at[1], nothing)
 
-    fresh = xs[layers].astype(F32)
-    square = jnp.sum(fresh * fresh, axis=1, keepdims=True)
+    square = jnp.zeros((rows, 1), F32)
+    for c in range(2):
+        fresh = xs[layers, c].astype(F32)
+        square = square + jnp.sum(fresh * fresh, axis=1, keepdims=True)
     sq_out[...] = jnp.broadcast_to(square, (rows, 128)).T[0:8]
 
     def sq_copy(d):
@@ -934,9 +985,12 @@
         total = total + sq_in[d, 0:1]
     inv = lax.rsqrt(total / full + EPSILON)
     inv = jnp.broadcast_to(inv, (128, rows)).T[:, 0:1]
-    out_ref[...] = (xs[layers].astype(F32) * inv * final_ref[...]).astype(BF16)
-
-    assert not end_line and not mid_in_line and not last_pieces
+    for c in range(2):
+        cols = slice(c * width, (c + 1) * width)
+        fresh = xs[layers, c].astype(F32)
+        out_ref[:, cols] = (fresh * inv * final_ref[:, cols]).astype(BF16)
+
+    assert not (end_line or mid_in_line or any(early) or any(final))
     close_weights()
 
     @at_end
@@ -992,7 +1046,6 @@
     sizes = (layers, n_sp, n_tp, n_grp, rows, chans, feats, depth, pieces)
     chips = n_tp // 2
     half_in = (layers, 2, depth // 2, chans)
-    half_out = (layers, 2, chans // 2, depth)
     vmem = pl.BlockSpec(memory_space=pltpu.VMEM)
     hbm = pl.BlockSpec(memory_space=pl.ANY)
     count = 3 * layers
@@ -1003,7 +1056,7 @@
         in_specs=[hbm] * 12,
         out_specs=vmem,
         scratch_shapes=[
-            pltpu.VMEM((rows, feats), BF16),
+            pltpu.VMEM((2, rows, feats // 2), BF16),
             pltpu.VMEM(filter_coefficients.shape, BF16),
             pltpu.VMEM(memory_valve_matrix.shape, BF16),
             pltpu.VMEM(entry_valve_matrix.shape, BF16),
@@ -1013,9 +1066,9 @@
             pltpu.VMEM((layers, n_tp * feats), F32),
             pltpu.VMEM((1, feats), F32),
             pltpu.VMEM((2 * layers * n_sp * 2, depth // 2, chans), BF16),
-            pltpu.VMEM((layers * n_sp * 2, chans // 2, depth), BF16),
-            pltpu.VMEM((layers + 1, n_tp, rows, feats), BF16),
-            pltpu.VMEM((layers + 1, rows, feats), BF16),
+            pltpu.VMEM((layers * n_sp * 2, chans, depth // 2), BF16),
+            pltpu.VMEM((layers + 1, n_tp, 2, rows, feats // 2), BF16),
+            pltpu.VMEM((layers + 1, 2, rows, feats // 2), BF16),
             pltpu.VMEM((rows, n_tp * feats), BF16),
             pltpu.VMEM((rows, n_tp * feats), BF16),
             pltpu.VMEM((layers, 8 + rows, chans), F32),
@@ -1026,18 +1079,18 @@
             pltpu.VMEM((rows, chans), BF16),
             pltpu.VMEM((len(LENT), rows, chans), BF16),
             pltpu.VMEM((len(LENT), rows, chans), BF16),
-            pltpu.VMEM((layers, n_tp, rows, feats), BF16),
-            pltpu.VMEM((layers, chips, rows, feats), BF16),
-            pltpu.VMEM((layers, chips, rows, feats), BF16),
-            pltpu.VMEM((layers, chips, rows, feats), BF16),
+            pltpu.VMEM((layers, n_tp, 2, rows, feats // 2), BF16),
+            pltpu.VMEM((layers, chips, 2, rows, feats // 2), BF16),
+            pltpu.VMEM((layers, chips, 2, rows, feats // 2), BF16),
+            pltpu.VMEM((layers, chips, 2, rows, feats // 2), BF16),
             pltpu.VMEM((layers, 2, chans), F32),
             pltpu.VMEM((layers, n_sp, 2, chans), F32),
             pltpu.VMEM((1, chans), F32),
             pltpu.VMEM((rows, 1), F32),
             pltpu.VMEM((8, rows), F32),
             pltpu.VMEM((n_tp, 8, rows), F32),
-            dma((9,)),
-            dma((count,)),
+            dma((10,)),
+            dma((count, 2)),
             dma((count, n_sp - 1, PARTS)),
             dma((count, n_sp - 1)),
             dma((3,)),
@@ -1059,7 +1112,7 @@
         starting_stream,
         multiplier_matrix.reshape(half_in),
         memory_path_matrix.reshape(half_in),
-        exit_projector_matrix.reshape(half_out),
+        exit_projector_matrix,
         filter_coefficients,
         memory_valve_matrix,
         entry_valve_matrix,
@@ -1083,7 +1136,7 @@
         and n_tp % 2 == 0
         and rows % 128 == 0
         and depth % 128 == 0
-        and feats % 128 == 0
+        and feats % 256 == 0
         and chans % BLOCK_W == 0
         and depth == feats
         and n_sp == n_tp

time: 113 us -> 110 us (0.973)
  Pallas kernels: 111 us -> 109 us
    pallas_call x1, Pallas kernels: 111 us -> 109 us  [in_one_kernel(): pl.pallas_call(functools.partial(fused, sizes), out_shape=jax.ShapeDtypeS...]
where the time goes in v4:
time: 110 us
  Pallas kernels  109 us (99%)
  local copies, waits for them, and re-layouts  1.77 us (2%)
    pallas_call x1, Pallas kernels, in_one_kernel(): pl.pallas_call(functools.partial(fused, sizes), out_shape=jax.ShapeDtypeS...  109 us

profile of v4, /device:TPU:0, one launch (start us, length us, event | category | flops | bytes accessed | tf_op | source)
XLA Modules:
  0.0 110.4 jit_solution(12028906391454568581)
XLA Ops:
  0.0 108.6 %shard_map.118 = bf16[384,512]{1,0:T(8,128)(2,1)} custom-call(bf16[384,512]{1,0:T(8,128)(2,1)} %x_hbm.1, bf16[2,2,256,512]{3,2,1,0:T(8,128)(2,1)} %bitcast.3, bf16[2,2,256,512]{3,2,1,0:T(8,128)(2,1)} %bitcast.4, bf16[2,512,512]{2,1,0:T(8,128)(2,1)} %exit_w.1, bf16[2,4,512]{2,1,0:T(4,128)(2,1)} %taps_hbm.1, bf16[2,2,256,256]{3,2,1,0:T(8,128)(2,1)} %reset_hbm.1, ...), custom_call_target="tpu_custom_call" | custom-call | tf_op jit(solution)/shard_map/pallas_call | solution.py:1053
  108.6 1.8 %copy.14 = bf16[384,512]{1,0:T(8,128)(2,1)} copy(bf16[384,512]{1,0:T(8,128)(2,1)} %shard_map.118) | data formatting | bytes 786432

commit v5 on v4

--- a/solution.py
+++ b/solution.py
@@ -910,9 +910,9 @@
     def rest_ahead(i, stage):
         even, odd = {
             (1, 0): (0, 1),
-            (1, 1): (0, 2),
-            (2, 0): (1, 1),
-            (3, 0): (1, 0),
+            (1, 1): (1, 2),
+            (1, 2): (1, 0),
+            (2, 0): (0, 1),
             (3, 1): (1, 1),
             (3, 2): (2, 1),
             (3, 3): (1, 0),
@@ -941,12 +941,13 @@
     pl.when(s == 1)(M(5, 2))
     end_next(final, 1, 1)
     take_halo(1)
+    end_next(final, 1, 0)
     gates(1, 0)
     end_next(final, 1, 1)
     gates(1, 1)
     send_carry(1)
     pl.when(is_mid & (s > 1))(M(5, 2))
-    end_next(final, 2, 1)
+    end_next(final, 1, 1)
     arrived(4)
     end_next(final, 1, 0)
     gel_s[...] = jax.nn.gelu(project(3, nrm).astype(F32))

time: 110 us -> 110 us (level)
  no operation moved by 1% of the time
where the time goes in v5:
time: 110 us
  Pallas kernels  108 us (98%)
  local copies, waits for them, and re-layouts  1.77 us (2%)
    pallas_call x1, Pallas kernels, in_one_kernel(): pl.pallas_call(functools.partial(fused, sizes), out_shape=jax.ShapeDtypeS...  108 us

profile of v5, /device:TPU:0, one launch (start us, length us, event | category | flops | bytes accessed | tf_op | source)
XLA Modules:
  0.0 109.6 jit_solution(7011197874614108441)
XLA Ops:
  0.0 107.8 %shard_map.118 = bf16[384,512]{1,0:T(8,128)(2,1)} custom-call(bf16[384,512]{1,0:T(8,128)(2,1)} %x_hbm.1, bf16[2,2,256,512]{3,2,1,0:T(8,128)(2,1)} %bitcast.3, bf16[2,2,256,512]{3,2,1,0:T(8,128)(2,1)} %bitcast.4, bf16[2,512,512]{2,1,0:T(8,128)(2,1)} %exit_w.1, bf16[2,4,512]{2,1,0:T(4,128)(2,1)} %taps_hbm.1, bf16[2,2,256,256]{3,2,1,0:T(8,128)(2,1)} %reset_hbm.1, ...), custom_call_target="tpu_custom_call" | custom-call | tf_op jit(solution)/shard_map/pallas_call | solution.py:1054
  107.8 1.8 %copy.14 = bf16[384,512]{1,0:T(8,128)(2,1)} copy(bf16[384,512]{1,0:T(8,128)(2,1)} %shard_map.118) | data formatting | bytes 786432
